TPU v7x, 128 devices: a whole 4x4x4 slice. The times are simulated.
128 devices in a mesh: sp: 16 (over z, y), dp: 8 (over x, core).
Axes of the slice: x: 4, y: 4, z: 4, core: 2. Of those that a mesh axis runs over, the one named last changes fastest.
Arguments:
- out_cotangent: bfloat16 [8, 4096, 2048], P('dp', 'sp'), may hold values from -6 to 6
- value_pre: bfloat16 [8, 4096, 2048], P('dp', 'sp'), may hold values from -8 to 8
- gate_pre: bfloat16 [8, 4096, 2048], P('dp', 'sp'), may hold values from -8 to 8
- out_weight: bfloat16 [2048, 2048], P('dp'), may hold values from -0.125 to 0.125
- conv_kernel: bfloat16 [31, 2048], P(None, 'sp'), may hold values from -6 to 6
- norm_gain: bfloat16 [2048], P('sp'), may hold values from 0.099609375 to 1.8984375
Outputs:
- grad_value: bfloat16 [8, 4096, 2048], P('dp', 'sp')
- grad_gate: bfloat16 [8, 4096, 2048], P('dp', 'sp')
- grad_out_weight: float32 [2048, 2048], P(('sp', 'dp'))
- grad_kernel: float32 [31, 2048], P(None, 'sp')
- grad_gain: float32 [2048], P('sp')
All inputs are finite; a program needn't handle non-finite values.
Results may differ from a plain program's by a relative error of at most 0.011.
Values may be sent and summed in bfloat16 or wider, within the bound.
A program may use at most 128 MiB of HBM per device.

v0:
```python
import jax
import jax.numpy as jnp
from jax import lax
from jax.sharding import PartitionSpec as P

epsilon = 1e-05


def rows_first(arrays, axis, dims):
    turned = [jnp.moveaxis(a, dim, 0) for a, dim in zip(arrays, dims)]
    both = jnp.concatenate([t.reshape(len(t), -1) for t in turned], axis=1)
    whole, at, outs = (lax.all_gather(both, axis, axis=0, tiled=True), 0, [])
    for t, dim in zip(turned, dims):
        piece = whole[:, at : at + t[0].size].reshape(-1, *t.shape[1:])
        outs.append(jnp.moveaxis(piece, 0, dim))
        at += t[0].size
    return tuple(outs)


def passed_along(value, axis, steps):
    count = lax.axis_size(axis)
    initial, last = (max(0, -steps), min(count, count - steps))
    return lax.ppermute(value, axis, [(source, source + steps) for source in range(initial, last)])


def cut_along(x, dim, devices):
    shape = x.shape
    blocks = x.reshape(*shape[:dim], devices, shape[dim] // devices, *shape[dim + 1 :])
    return jnp.moveaxis(blocks, dim, 0)


def summed_on_arrival(x, axis, dim):
    devices = lax.axis_size(axis)
    blocks = lax.all_to_all(cut_along(x, dim, devices), axis, 0, 0, tiled=True)
    return jnp.sum(blocks, axis=0)


def copy_for_each(x, axis):
    devices = lax.axis_size(axis)
    return lax.all_to_all(jnp.broadcast_to(x[None], (devices, *x.shape)), axis, 0, 0, tiled=True)


def of_everyone(x, axis):
    return copy_for_each(x, axis).sum(axis=0)


def packed_total(arrays, axis):
    vector, at, outs = (jnp.concatenate([a.reshape(-1) for a in arrays]), 0, [])
    total = of_everyone(vector, axis)
    for a in arrays:
        outs.append(total[at : at + a.size].reshape(a.shape))
        at += a.size
    return tuple(outs)


def sum_at_owner(x, axis, dim):
    devices = lax.axis_size(axis)
    blocks = lax.all_to_all(cut_along(x, dim, devices), axis, 0, 0, tiled=True)
    return jnp.sum(blocks.astype(jnp.float32), axis=0)


def gated_forward(values_in, gates_in):
    return (values_in.astype(jnp.float32) * jax.nn.sigmoid(gates_in.astype(jnp.float32))).astype(
        jnp.bfloat16
    )


def gated_backward(grad_gated, values_in, gates_in):
    sigmoid_gate = jax.nn.sigmoid(gates_in.astype(jnp.float32))
    grad_float = grad_gated.astype(jnp.float32)
    grad_values = (grad_float * sigmoid_gate).astype(jnp.bfloat16)
    grad_gates = (
        grad_float * values_in.astype(jnp.float32) * sigmoid_gate * (1.0 - sigmoid_gate)
    ).astype(jnp.bfloat16)
    return (grad_values, grad_gates)


def local_sums(first, second):
    return (first, second)


def mechanism(
    gated, front_rows, grad_act, kernel, gain, channel_count, moments_fn, grad_moments_fn, after_fn
):
    taps_count = kernel.shape[0]
    row_count = gated.shape[0]
    taps_float = kernel.astype(jnp.float32)
    gain_float = gain.astype(jnp.float32)
    extended = jnp.concatenate([front_rows, gated], axis=0).astype(jnp.float32)
    conv = jnp.zeros((row_count, gated.shape[1]), jnp.float32)
    for offset in range(taps_count):
        begin = taps_count - 1 - offset
        conv = conv + taps_float[offset] * extended[begin : begin + row_count]
    total, squares = moments_fn(jnp.sum(conv, axis=1), jnp.sum(conv * conv, axis=1))
    centre = (total / channel_count)[:, None]
    variance = (squares / channel_count)[:, None] - centre * centre
    inv_scale = lax.rsqrt(variance + epsilon)
    centred = (conv - centre) * inv_scale
    normed = centred * gain_float
    sig_norm = jax.nn.sigmoid(normed)
    activation = (normed * sig_norm).astype(jnp.bfloat16)
    grad_normed = grad_act.astype(jnp.float32) * sig_norm * (1.0 + normed * (1.0 - sig_norm))
    gain_part = jnp.sum(grad_normed * centred, axis=0)
    grad_centred = grad_normed * gain_float
    first, second = grad_moments_fn(
        jnp.sum(grad_centred, axis=1), jnp.sum(grad_centred * centred, axis=1)
    )
    grad_conv = (
        grad_centred
        - (first / channel_count)[:, None]
        - centred * (second / channel_count)[:, None]
    ) * inv_scale
    grad_extended = jnp.concatenate([grad_conv, after_fn(grad_conv, taps_count)], axis=0)
    grad_gated = jnp.zeros(grad_conv.shape, jnp.float32)
    kernel_rows = []
    for offset in range(taps_count):
        grad_gated = grad_gated + taps_float[offset] * grad_extended[offset : offset + row_count]
        begin = taps_count - 1 - offset
        kernel_rows.append(jnp.sum(grad_conv * extended[begin : begin + row_count], axis=0))
    return (activation, grad_gated.astype(jnp.bfloat16), jnp.stack(kernel_rows, axis=0), gain_part)


def shards(out_cotangent, value_pre, gate_pre, out_weight, conv_kernel, norm_gain):
    cotangent = out_cotangent[0]
    values_in = value_pre[0]
    gates_in = gate_pre[0]
    row_count = cotangent.shape[0]
    taps_count = conv_kernel.shape[0]
    width_all = cotangent.shape[1]
    grad_act = lax.dot_general(
        cotangent,
        lax.all_gather(out_weight, "dp", axis=0, tiled=True),
        (((1,), (1,)), ((), ())),
        preferred_element_type=jnp.float32,
    ).astype(jnp.bfloat16)
    kernel_all, gain_all = rows_first((conv_kernel, norm_gain), "sp", (1, 0))
    gated = gated_forward(values_in, gates_in)
    front_rows = passed_along(gated[row_count - taps_count + 1 :], "sp", 1)

    def later_margin(grad_conv, count_taps):
        return passed_along(grad_conv[: count_taps - 1], "sp", -1)

    activation, grad_gated, kernel_full, gain_full = mechanism(
        gated,
        front_rows,
        grad_act,
        kernel_all,
        gain_all,
        float(width_all),
        local_sums,
        local_sums,
        later_margin,
    )
    kernel_part, gain_part = (
        summed_on_arrival(kernel_full, "sp", 1),
        summed_on_arrival(gain_full, "sp", 0),
    )
    grad_values, grad_gates = gated_backward(grad_gated, values_in, gates_in)
    token_total = lax.axis_size("sp") * lax.axis_size("dp") * row_count
    factor = float(token_total) ** (-0.5)
    kernel_sum, gain_sum = packed_total((kernel_part, gain_part), "dp")
    partial_sum = lax.psum_scatter(
        lax.dot_general(
            activation, cotangent, (((0,), (0,)), ((), ())), preferred_element_type=jnp.float32
        ).astype(jnp.bfloat16),
        "sp",
        scatter_dimension=0,
        tiled=True,
    )
    weight_sum = sum_at_owner(partial_sum, "dp", 0)
    return (
        grad_values[None],
        grad_gates[None],
        weight_sum * factor,
        kernel_sum * factor,
        gain_sum * factor,
    )


def solution(mesh):
    placed = (
        P("dp", "sp", None),
        P("dp", "sp", None),
        P("dp", "sp", None),
        P("dp", None),
        P(None, "sp"),
        P("sp"),
    )
    return jax.shard_map(
        shards,
        mesh=mesh,
        in_specs=placed,
        out_specs=(
            P("dp", "sp", None),
            P("dp", "sp", None),
            P(("sp", "dp"), None),
            P(None, "sp"),
            P("sp"),
        ),
        check_vma=False,
    )
```

profile of v0, /device:TPU:1, one launch (start us, length us, event | category | flops | bytes accessed | tf_op | source)
XLA Modules:
  0.0 170.3 jit_solution(999146623996207987)
XLA Ops:
  8.8 2.1 %fusion.93 = bf16[256,2048]{1,0:T(8,128)(2,1)S(1)} fusion(bf16[1,256,2048]{2,1,0:T(8,128)(2,1)} %param.7, bf16[1,256,2048]{2,1,0:T(8,128)(2,1)} %param.8), kind=kLoop, calls=%fused_computation.156 | loop fusion | flops 3670016 | bytes 3145728 | tf_op jit(solution)/shard_map/convert_element_type | solution.py:63
  11.0 4.0 %collective-permute-start = (bf16[30,2048]{1,0:T(8,128)(2,1)S(1)}, bf16[30,2048]{1,0:T(8,128)(2,1)S(1)}, u32[]{:S(2)}, u32[]{:S(2)}) collective-permute-start(bf16[30,2048]{1,0:T(8,128)(2,1)S(1)} %slice.464), channel_id=1, source_target_pairs={{0,8},{8,16},{16,24},{24,32},{32,40},{40,48},{48,56},{56,64},{64,7... | collective-permute-start | bytes 368648 | tf_op jit(solution)/shard_map/ppermute | solution.py:23
  15.1 20.8 %all_gather.6 = bf16[2048,32]{0,1:T(8,128)(2,1)S(1)} all-gather(bf16[128,32]{0,1:T(8,128)(2,1)S(1)} %pad_maximum_fusion.2), channel_id=1, replica_groups=mesh['sp'=16,'dp'=8] {'sp'}, dimensions={0}, use_global_device_ids=true | all-gather | bytes 139264 | tf_op jit(solution)/shard_map/all_gather | solution.py:12
  36.6 11.0 %fusion.108 = (f32[256]{0:T(256)S(1)}, f32[256]{0:T(256)S(1)}, f32[256,2048]{1,0:T(8,128)S(1)}) fusion(f32[286,2048]{1,0:T(8,128)S(1)} %maximum_convert_fusion, f32[2048]{0:T(1024)S(1)} %bitcast.128, f32[2048]{0:T(1024)S(1)} %bitcast.130, f32[2048]{0:T(1024)S(1)} %bitcast.132, f32[2048]{0:T(1024)S(1)} %bitcast.134, f32[2048]{0:T(1024)S(1)} %bitcast.136, ...), kind=kLoop, calls=%fused_computation.227 | loop fusion | flops 33553920 | bytes 67364864 | tf_op jit(solution)/shard_map/reduce_sum | solution.py:94
  47.8 1.3 copy-done.3
  49.1 6.0 %convolution_convert_fusion = bf16[2048,2048]{1,0:T(8,128)(2,1)} fusion(f32[256,2048]{1,0:T(8,128)S(1)} %get-tuple-element.44, bf16[1,256,2048]{2,1,0:T(8,128)(2,1)S(1)} %copy-done, f32[2048]{0:T(1024)S(1)} %bitcast.196, f32[256]{0:T(256)S(1)} %get-tuple-element.77, f32[256]{0:T(256)S(1)} %get-tuple-element.76), kind=kOutput, calls=%fused_computation.29 | convolution fusion | flops 2155872256 | bytes 11544576 | tf_op jit(solution)/shard_map/dot_general | solution.py:163
  55.2 8.6 %all-gather.2.cloned.1.call-done = bf16[2048,2048]{1,0:T(8,128)(2,1)} async-done(((bf16[256,2048]{1,0:T(8,128)(2,1)}), bf16[2048,2048]{1,0:T(8,128)(2,1)}) %all-gather.2.cloned.1.call-update) | async-done | bytes 8388624 | tf_op jit(solution)/shard_map/all_gather | solution.py:132
  63.8 9.1 %multiply_reduce_fusion = (f32[2048]{0:T(1024)}, f32[256]{0:T(256)}, f32[256]{0:T(256)}, f32[256,2048]{1,0:T(8,128)}) fusion(f32[256,2048]{1,0:T(8,128)} %copy-done.3, f32[256]{0:T(256)} %copy-done.20, f32[256]{0:T(256)} %copy-done.19, f32[2048]{0:T(1024)} %bitcast.197, bf16[2048,2048]{1,0:T(8,128)(2,1)} %all-gather.2.cloned.1.call-done, ...), kind=kOutput, calls=%fused_computation.163 | convolution fusion | flops 2157442560 | bytes 13651968 | tf_op jit(solution)/shard_map/dot_general | solution.py:130
  73.0 6.8 %all-to-all-start.2 = ((f32[16,1,128]{2,1,0:T(1,128)}), f32[16,1,128]{2,1,0:T(1,128)}, u32[]{:S(2)}, u32[]{:S(2)}) async-start(f32[16,1,128]{2,1,0:T(1,128)} %bitcast.200), calls=%async_computation.3 | async-start | bytes 16384 | tf_op jit(solution)/shard_map/all_to_all | solution.py:34
  80.4 8.2 %multiply_reduce_fusion.1 = (f32[2048]{0:T(1024)}, f32[2048]{0:T(1024)}, f32[2048]{0:T(1024)}, f32[2048]{0:T(1024)}, f32[2048]{0:T(1024)}, /*index=5*/f32[2048]{...) fusion(f32[286,2048]{1,0:T(8,128)S(1)} %maximum_convert_fusion,, ...), kind=kLoop, calls=%fused_computation.164 | loop fusion | flops 22507520 | bytes 44199936 | tf_op jit(solution)/shard_map/reduce_sum | solution.py:119
  88.6 4.7 %multiply_reduce_fusion.19 = (f32[2048]{0:T(1024)}, f32[2048]{0:T(1024)}, f32[2048]{0:T(1024)}, f32[2048]{0:T(1024)}, f32[2048]{0:T(1024)}, /*index=5*/f32[2048]...) fusion(f32[256,2048]{1,0:T(8,128)S(1)} %get-tuple-element.41, ...), kind=kLoop, calls=%fused_computation.182 | loop fusion | flops 13604864 | bytes 29466624 | tf_op jit(solution)/shard_map/reduce_sum | solution.py:119
  93.4 6.3 %stack.127 = f32[31,16,128]{2,0,1:T(8,128)} concatenate(f32[1,16,128]{2,0,1:T(1,128)} %bitcast.195, f32[1,16,128]{2,0,1:T(1,128)} %bitcast.194, f32[1,16,128]{2,0,1:T(1,128)} %bitcast.193, f32[1,16,128]{2,0,1:T(1,128)} %bitcast.192, f32[1,16,128]{2,0,1:T(1,128)} %bitcast.191, f32[1,16,128]{2,0,1:T(1,128)} %bitcast.190, f32[1,16,128]{2,0,1:T(1,128)} %bitcast.189, ...), dimensions={0} | concatenate | bytes 507904 | tf_op jit(solution)/shard_map/stack | solution.py:120
  99.7 6.6 %all-to-all-start.1 = ((f32[16,31,128]{2,1,0:T(8,128)}), f32[16,31,128]{2,1,0:T(8,128)S(1)}, u32[]{:S(2)}, u32[]{:S(2)}) async-start(f32[16,31,128]{2,1,0:T(8,128)} %bitcast.73), calls=%async_computation.2 | async-start | bytes 524288 | tf_op jit(solution)/shard_map/all_to_all | solution.py:34
  106.2 1.7 slice.527
  107.9 1.3 collective-permute-start.1
  109.2 1.2 reduce_sum.398
  110.4 5.9 %all-to-all-done.1 = f32[16,31,128]{2,1,0:T(8,128)S(1)} async-done(((f32[16,31,128]{2,1,0:T(8,128)}), f32[16,31,128]{2,1,0:T(8,128)S(1)}, u32[]{:S(2)}, u32[]{:S(2)}) %all-to-all-start.1) | async-done | bytes 253984 | tf_op jit(solution)/shard_map/all_to_all | solution.py:34
  117.0 0.7 pad_maximum_fusion.1
  118.4 5.9 %all-to-all-start.3 = ((f32[8,1,4096]{2,1,0:T(1,128)}), f32[8,1,4096]{2,1,0:T(1,128)S(1)}, u32[]{:S(2)}, u32[]{:S(2)}) async-start(f32[8,1,4096]{2,1,0:T(1,128)} %broadcast_in_dim.8), calls=%async_computation.4 | async-start | bytes 262144 | tf_op jit(solution)/shard_map/all_to_all | solution.py:40
  124.3 16.4 %fusion.98 = (bf16[1,256,2048]{2,1,0:T(8,128)(2,1)}, bf16[256,2048]{1,0:T(8,128)(2,1)}) fusion(bf16[1,256,2048]{2,1,0:T(8,128)(2,1)} %param.7, bf16[1,256,2048]{2,1,0:T(8,128)(2,1)} %param.8, f32[30,2048]{1,0:T(8,128)} %collective-permute-done.1, f32[256,2048]{1,0:T(8,128)S(1)} %copy-done.2, f32[2048]{0:T(1024)S(1)} %bitcast.129, f32[2048]{0:T(1024)S(1)} %bitcast.131, ...), kind=kLoop, calls=%fused_computation.205 | loop fusion | flops 54001664 | bytes 6791168 | tf_op jit(solution)/shard_map/broadcast_in_dim | solution.py:173
  140.7 5.6 %reduce-scatter.2.cloned.1.call-done = bf16[128,2048]{1,0:T(8,128)(2,1)} async-done(((bf16[2048,2048]{1,0:T(8,128)(2,1)}), bf16[128,2048]{1,0:T(8,128)(2,1)}) %reduce-scatter.2.cloned.1.call-update) | async-done | bytes 524304 | tf_op jit(solution)/shard_map/reduce_scatter | solution.py:162
  146.4 6.4 %all-to-all-start = ((bf16[8,16,2048]{2,1,0:T(8,128)(2,1)}), bf16[8,16,2048]{2,1,0:T(8,128)(2,1)S(1)}, u32[]{:S(2)}, u32[]{:S(2)}) async-start(bf16[8,16,2048]{2,1,0:T(8,128)(2,1)} %bitcast.101), calls=%async_computation.1 | async-start | bytes 1048576 | tf_op jit(solution)/shard_map/all_to_all | solution.py:58
  152.8 3.1 %fusion.99 = bf16[1,256,2048]{2,1,0:T(8,128)(2,1)} fusion(bf16[256,2048]{1,0:T(8,128)(2,1)} %get-tuple-element.43, bf16[1,256,2048]{2,1,0:T(8,128)(2,1)} %param.8), kind=kLoop, calls=%fused_computation.206 | loop fusion | flops 3670016 | bytes 3145728 | tf_op jit(solution)/shard_map/broadcast_in_dim | solution.py:172
  157.1 5.0 %all-to-all-done = bf16[8,16,2048]{2,1,0:T(8,128)(2,1)S(1)} async-done(((bf16[8,16,2048]{2,1,0:T(8,128)(2,1)}), bf16[8,16,2048]{2,1,0:T(8,128)(2,1)S(1)}, u32[]{:S(2)}, u32[]{:S(2)}) %all-to-all-start) | async-done | bytes 524320 | tf_op jit(solution)/shard_map/all_to_all | solution.py:58
  (67 shorter events, 5.5 us)
Async XLA Ops:
  8.0 41.1 %copy-start = (bf16[1,256,2048]{2,1,0:T(8,128)(2,1)S(1)}, bf16[1,256,2048]{2,1,0:T(8,128)(2,1)}, u32[]{:S(2)}) copy-start(bf16[1,256,2048]{2,1,0:T(8,128)(2,1)} %param.6) | copy-start | bytes 3145732
  8.0 55.8 %all-gather.2.cloned.1.call-start = ((), (), s32[]{:S(2)}) async-start(), calls=%async_computation.5 | async-start | bytes 9437184 | tf_op jit(solution)/shard_map/all_gather | solution.py:132
  8.8 137.6 %reduce-scatter.2.cloned.1.call-start = ((), (), s32[]{:S(2)}) async-start(), calls=%async_computation.6 | async-start | bytes 8912896 | tf_op jit(solution)/shard_map/reduce_scatter | solution.py:162
  11.0 25.3 %collective-permute-start = (bf16[30,2048]{1,0:T(8,128)(2,1)S(1)}, bf16[30,2048]{1,0:T(8,128)(2,1)S(1)}, u32[]{:S(2)}, u32[]{:S(2)}) collective-permute-start(bf16[30,2048]{1,0:T(8,128)(2,1)S(1)} %slice.464), channel_id=1, source_target_pairs={{0,8},{8,16},{16,24},{24,32},{32,40},{40,48},{48,56},{56,64},{64,7... | collective-permute-start | bytes 368648 | tf_op jit(solution)/shard_map/ppermute | solution.py:23
  36.1 11.5 %copy-start.4 = (f32[1,2048]{1,0:T(1,128)}, f32[1,2048]{1,0:T(1,128)S(1)}, u32[]{:S(2)}) copy-start(f32[1,2048]{1,0:T(1,128)S(1)} %get-tuple-element.51) | copy-start | bytes 24580
  36.1 11.5 %copy-start.5 = (f32[1,2048]{1,0:T(1,128)}, f32[1,2048]{1,0:T(1,128)S(1)}, u32[]{:S(2)}) copy-start(f32[1,2048]{1,0:T(1,128)S(1)} %get-tuple-element.52) | copy-start | bytes 24580
  36.1 11.5 %copy-start.6 = (f32[1,2048]{1,0:T(1,128)}, f32[1,2048]{1,0:T(1,128)S(1)}, u32[]{:S(2)}) copy-start(f32[1,2048]{1,0:T(1,128)S(1)} %get-tuple-element.53) | copy-start | bytes 24580
  36.1 11.5 %copy-start.7 = (f32[1,2048]{1,0:T(1,128)}, f32[1,2048]{1,0:T(1,128)S(1)}, u32[]{:S(2)}) copy-start(f32[1,2048]{1,0:T(1,128)S(1)} %get-tuple-element.54) | copy-start | bytes 24580
  36.2 11.5 %copy-start.8 = (f32[1,2048]{1,0:T(1,128)}, f32[1,2048]{1,0:T(1,128)S(1)}, u32[]{:S(2)}) copy-start(f32[1,2048]{1,0:T(1,128)S(1)} %get-tuple-element.55) | copy-start | bytes 24580
  36.2 11.5 %copy-start.9 = (f32[1,2048]{1,0:T(1,128)}, f32[1,2048]{1,0:T(1,128)S(1)}, u32[]{:S(2)}) copy-start(f32[1,2048]{1,0:T(1,128)S(1)} %get-tuple-element.56) | copy-start | bytes 24580
  36.2 11.5 %copy-start.10 = (f32[1,2048]{1,0:T(1,128)}, f32[1,2048]{1,0:T(1,128)S(1)}, u32[]{:S(2)}) copy-start(f32[1,2048]{1,0:T(1,128)S(1)} %get-tuple-element.57) | copy-start | bytes 24580
  36.2 11.5 %copy-start.11 = (f32[1,2048]{1,0:T(1,128)}, f32[1,2048]{1,0:T(1,128)S(1)}, u32[]{:S(2)}) copy-start(f32[1,2048]{1,0:T(1,128)S(1)} %get-tuple-element.58) | copy-start | bytes 24580
  36.2 11.5 %copy-start.12 = (f32[1,2048]{1,0:T(1,128)}, f32[1,2048]{1,0:T(1,128)S(1)}, u32[]{:S(2)}) copy-start(f32[1,2048]{1,0:T(1,128)S(1)} %get-tuple-element.59) | copy-start | bytes 24580
  36.2 11.5 %copy-start.13 = (f32[1,2048]{1,0:T(1,128)}, f32[1,2048]{1,0:T(1,128)S(1)}, u32[]{:S(2)}) copy-start(f32[1,2048]{1,0:T(1,128)S(1)} %get-tuple-element.60) | copy-start | bytes 24580
  36.2 11.5 %copy-start.14 = (f32[1,2048]{1,0:T(1,128)}, f32[1,2048]{1,0:T(1,128)S(1)}, u32[]{:S(2)}) copy-start(f32[1,2048]{1,0:T(1,128)S(1)} %get-tuple-element.61) | copy-start | bytes 24580
  36.2 11.5 %copy-start.15 = (f32[1,2048]{1,0:T(1,128)}, f32[1,2048]{1,0:T(1,128)S(1)}, u32[]{:S(2)}) copy-start(f32[1,2048]{1,0:T(1,128)S(1)} %get-tuple-element.62) | copy-start | bytes 24580
  36.2 11.5 %copy-start.16 = (f32[1,2048]{1,0:T(1,128)}, f32[1,2048]{1,0:T(1,128)S(1)}, u32[]{:S(2)}) copy-start(f32[1,2048]{1,0:T(1,128)S(1)} %get-tuple-element.63) | copy-start | bytes 24580
  36.3 11.5 %copy-start.17 = (f32[2048,1]{0,1:T(1,128)}, f32[2048,1]{0,1:T(1,128)S(1)}, u32[]{:S(2)}) copy-start(f32[2048,1]{0,1:T(1,128)S(1)} %slice_convert_fusion) | copy-start | bytes 24580
  73.0 26.7 %all-to-all-start.2 = ((f32[16,1,128]{2,1,0:T(1,128)}), f32[16,1,128]{2,1,0:T(1,128)}, u32[]{:S(2)}, u32[]{:S(2)}) async-start(f32[16,1,128]{2,1,0:T(1,128)} %bitcast.200), calls=%async_computation.3 | async-start | bytes 16384 | tf_op jit(solution)/shard_map/all_to_all | solution.py:34
  93.4 31.0 %copy-start.2 = (f32[256,2048]{1,0:T(8,128)S(1)}, f32[256,2048]{1,0:T(8,128)}, u32[]{:S(2)}) copy-start(f32[256,2048]{1,0:T(8,128)} %copy-done.1) | copy-start | bytes 6291460
  99.7 16.7 %all-to-all-start.1 = ((f32[16,31,128]{2,1,0:T(8,128)}), f32[16,31,128]{2,1,0:T(8,128)S(1)}, u32[]{:S(2)}, u32[]{:S(2)}) async-start(f32[16,31,128]{2,1,0:T(8,128)} %bitcast.73), calls=%async_computation.2 | async-start | bytes 524288 | tf_op jit(solution)/shard_map/all_to_all | solution.py:34
  107.9 16.4 %collective-permute-start.1 = (f32[30,2048]{1,0:T(8,128)}, f32[30,2048]{1,0:T(8,128)}, u32[]{:S(2)}, u32[]{:S(2)}) collective-permute-start(f32[30,2048]{1,0:T(8,128)} %slice.527), channel_id=1, source_target_pairs={{8,0},{16,8},{24,16},{32,24},{40,32},{48,40},{56,48},{64,56},{72,6... | collective-permute-start | bytes 737288 | tf_op jit(solution)/shard_map/ppermute | solution.py:23
  118.4 22.3 %all-to-all-start.3 = ((f32[8,1,4096]{2,1,0:T(1,128)}), f32[8,1,4096]{2,1,0:T(1,128)S(1)}, u32[]{:S(2)}, u32[]{:S(2)}) async-start(f32[8,1,4096]{2,1,0:T(1,128)} %broadcast_in_dim.8), calls=%async_computation.4 | async-start | bytes 262144 | tf_op jit(solution)/shard_map/all_to_all | solution.py:40
  146.4 15.7 %all-to-all-start = ((bf16[8,16,2048]{2,1,0:T(8,128)(2,1)}), bf16[8,16,2048]{2,1,0:T(8,128)(2,1)S(1)}, u32[]{:S(2)}, u32[]{:S(2)}) async-start(bf16[8,16,2048]{2,1,0:T(8,128)(2,1)} %bitcast.101), calls=%async_computation.1 | async-start | bytes 1048576 | tf_op jit(solution)/shard_map/all_to_all | solution.py:58
  (6 other events, 22.8 us)
Sparse Core Ops, SparseCore 0:
  10.6 53.2 all-gather.1
Sparse Core Ops, SparseCore 1:
  55.3 91.0 reduce-scatter.1
where the time goes:
time: 172 us; the launch traced here: 170 us
  other arithmetic  51.2 us (30%)
  starting transfers between devices  31 us (18%)
  waiting for transfers between devices  25.9 us (15%)
  blocking collectives  20.8 us (12%)
  between operations  15.9 us (9%)
  matrix products  15.2 us (9%)
  local copies, waits for them, and re-layouts  10.3 us (6%)
    all_gather x1, blocking collectives, rows_first(): whole, at, outs = (lax.all_gather(both, axis, axis=0, tiled=True), 0, [])  20.8 us
    broadcast_in_dim x1, other arithmetic, shards(): grad_gates[None]  16.4 us
    all_to_all x2, starting transfers between devices, summed_on_arrival(): blocks = lax.all_to_all(cut_along(x, dim, devices), axis, 0, 0, tiled=True)  13.3 us
    reduce_sum x2, other arithmetic, mechanism(): jnp.sum(grad_conv * extended[begin:begin + row_count], axis=0)  12.9 us
    reduce_sum x1, other arithmetic, mechanism(): jnp.sum(conv, axis=1)  11 us
    dot_general x1, matrix products, shards(): lax.dot_general(cotangent, lax.all_gather(out_weight, 'dp', axis=0, tiled...  9.14 us
    all_gather x1, waiting for transfers between devices, shards(): lax.all_gather(out_weight, 'dp', axis=0, tiled=True)  8.64 us
    all_to_all x1, starting transfers between devices, sum_at_owner(): blocks = lax.all_to_all(cut_along(x, dim, devices), axis, 0, 0, tiled=True)  6.4 us
  transfers between devices with their start and end apart: 8, of which 4 were waited for; matrix products, arithmetic and copies ran while one was open for 44% of the time, Pallas kernels for 0%

commit v1 on v0

v1 whole, which is shorter than its diff:
```python
import functools

import jax
import jax.numpy as jnp
from jax import lax
from jax.experimental import pallas as pl
from jax.experimental.pallas import tpu as pltpu
from jax.sharding import PartitionSpec as P

EPS = 1e-05
F32 = jnp.float32
BF16 = jnp.bfloat16
MESH = pl.DeviceIdType.MESH

ROWS = 256
SEG = 32
D = 2048
HALF = 1024
TAPS = 31
NSP = 16
NDP = 8
COLOURS = ((0, 384), (384, 384), (768, 256))

TAP0 = 0
COT0 = TAP0 + 16
HALO0 = COT0 + 1
WX0 = HALO0 + 1
WY0 = WX0 + 8
WZ0 = WY0 + 12
ACT0 = WZ0 + 12
GA0 = ACT0 + 4
RA0 = GA0 + 4
RB0 = RA0 + 18
RC0 = RB0 + 9
GK0 = RC0 + 9
GD0 = GK0 + 16
GC0 = GD0 + 8
FIN0 = GC0 + 1
NSEM = FIN0 + 1


def sigmoid(x):
    return 0.5 * jnp.tanh(0.5 * x) + 0.5


def lanes(i, n=128):
    return pl.ds(pl.multiple_of(i * n, n), n)


def rows(i, n):
    return pl.ds(pl.multiple_of(i * n, n), n)


def loop(n, body):
    def step(i, c):
        body(i)
        return c

    lax.fori_loop(0, n, step, 0)


def kernel(
    cot_hbm,
    val_hbm,
    gate_hbm,
    w_hbm,
    taps_in,
    gain_in,
    gv_hbm,
    gg_hbm,
    ow_ref,
    gk_ref,
    cotraw,
    cotp,
    val,
    gate,
    sig,
    gext,
    ext,
    cen,
    fwd,
    act,
    wg,
    ga,
    tkown,
    tkall,
    tkf,
    sum1,
    sum2,
    inv_b,
    hal,
    halr,
    ggp,
    gvo,
    ggo,
    gkp,
    gkr,
    gdo,
    gdr,
    pa,
    pb,
    pc,
    r1a,
    r1b,
    r1c,
    cba,
    cbb,
    cbc,
    s1a,
    s1b,
    s1c,
    r2a,
    r2b,
    r2c,
    s2a,
    s2b,
    s2c,
    r3a,
    r3b,
    r3c,
    finp,
    fins,
    finr,
    perm,
    permt,
    ssem,
    rsem,
    lsem,
):
    s = lax.axis_index("sp")
    d = lax.axis_index("dp")
    z, y = s // 4, s % 4
    x, q = d // 2, d % 2

    def at(axis, off):
        if axis == 0:
            return {"sp": s, "dp": ((x + off) % 4) * 2 + q}
        if axis == 1:
            return {"sp": z * 4 + (y + off) % 4, "dp": d}
        return {"sp": ((z + off) % 4) * 4 + y, "dp": d}

    partner = {"sp": s, "dp": x * 2 + (1 - q)}
    coord = (x, y, z)

    sent = []

    def copy(src, dst, i, dev):
        return pltpu.make_async_remote_copy(
            src_ref=src, dst_ref=dst, send_sem=ssem.at[i], recv_sem=rsem.at[i], device_id=dev, device_id_type=MESH
        )

    def send(src, dst, i, dev):
        c = copy(src, dst, i, dev)
        c.start()
        sent.append(c)

    def got(dst, i):
        copy(dst, dst, i, partner).wait_recv()

    local = [
        pltpu.make_async_copy(w_hbm, wg.at[x], lsem.at[0]),
        pltpu.make_async_copy(val_hbm, val, lsem.at[1]),
        pltpu.make_async_copy(gate_hbm, gate, lsem.at[2]),
        pltpu.make_async_copy(cot_hbm, cotraw.at[q], lsem.at[3]),
    ]
    for c in local:
        c.start()
    barrier = pltpu.get_barrier_semaphore()

    def greet_sp(r):
        pl.semaphore_signal(barrier, inc=1, device_id={"sp": (s + r + 1) % NSP, "dp": d}, device_id_type=MESH)

    def greet_dp(r):
        pl.semaphore_signal(barrier, inc=1, device_id={"sp": s, "dp": (d + r + 1) % NDP}, device_id_type=MESH)

    loop(NSP - 1, greet_sp)
    loop(NDP - 1, greet_dp)
    tkown[0:TAPS, :] = taps_in[...].astype(F32)
    tkown[TAPS : TAPS + 1, :] = gain_in[...].astype(F32)
    tkall[s] = tkown[...].astype(BF16)
    r_io = lax.broadcasted_iota(jnp.int32, (ROWS, ROWS), 0)
    t_io = lax.broadcasted_iota(jnp.int32, (ROWS, ROWS), 1)
    perm[...] = jnp.where(t_io == (r_io & 7) * SEG + (r_io >> 3), 1.0, 0.0).astype(BF16)
    permt[...] = jnp.where(r_io == (t_io & 7) * SEG + (t_io >> 3), 1.0, 0.0).astype(BF16)
    pl.semaphore_wait(barrier, NSP - 1 + NDP - 1)

    def wy(xx, yy, h=None):
        if h is None:
            return wg.at[xx, pl.ds(pl.multiple_of(yy * 64, 64), 64), pl.ds(0, HALF)]
        return wg.at[xx, pl.ds(pl.multiple_of(yy * 64 + h * 32, 32), 32), pl.ds(0, HALF)]

    def wz(xx, zz, h=None):
        if h is None:
            return wg.at[xx, pl.ds(pl.multiple_of(zz * 64, 64), 64), pl.ds(HALF, HALF)]
        return wg.at[xx, pl.ds(pl.multiple_of(zz * 64 + h * 32, 32), 32), pl.ds(HALF, HALF)]

    local[0].wait()
    for i, off in ((0, 1), (1, -1)):
        send(wy(x, y), wy(x, y), WX0 + i, at(0, off))
        send(wz(x, z), wz(x, z), WX0 + 2 + i, at(0, off))

    def send_taps(r):
        copy(tkall.at[s], tkall.at[s], TAP0 + r, {"sp": (s + r + 1) % NSP, "dp": d}).start()

    loop(NSP - 1, send_taps)

    local[1].wait()
    local[2].wait()

    def gate_block(i):
        at_rows = rows(ROWS // 32 - 1 - i, 32)
        sg = sigmoid(gate[at_rows, :].astype(F32))
        sig[at_rows, :] = sg
        gext[pl.ds(pl.multiple_of((ROWS // 32 - i) * 32, 32), 32), :] = (val[at_rows, :].astype(F32) * sg).astype(BF16)

    gate_block(0)

    def halo_copy():
        return copy(gext.at[pl.ds(ROWS, 32)], gext.at[pl.ds(0, 32)], HALO0, {"sp": (s + 1) % NSP, "dp": d})

    @pl.when(s < NSP - 1)
    def _():
        halo_copy().start()

    local[3].wait()
    send(cotraw.at[q], cotraw.at[q], COT0, partner)
    loop(ROWS // 32 - 1, lambda i: gate_block(i + 1))

    def weights_on(xx, pos):
        for i, off in ((0, 1), (1, -1)):
            send(wy(xx, y), wy(xx, y), WY0 + 4 * pos + i, at(1, off))
            send(wz(xx, z), wz(xx, z), WZ0 + 4 * pos + i, at(2, off))

    def weights_far(xx, pos):
        got(wy(xx, (y + 3) % 4), WY0 + 4 * pos)
        send(wy(xx, (y + 3) % 4, 0), wy(xx, (y + 3) % 4, 0), WY0 + 4 * pos + 2, at(1, 1))
        got(wz(xx, (z + 3) % 4), WZ0 + 4 * pos)
        send(wz(xx, (z + 3) % 4, 0), wz(xx, (z + 3) % 4, 0), WZ0 + 4 * pos + 2, at(2, 1))
        got(wy(xx, (y + 1) % 4), WY0 + 4 * pos + 1)
        send(wy(xx, (y + 1) % 4, 1), wy(xx, (y + 1) % 4, 1), WY0 + 4 * pos + 3, at(1, -1))
        got(wz(xx, (z + 1) % 4), WZ0 + 4 * pos + 1)
        send(wz(xx, (z + 1) % 4, 1), wz(xx, (z + 1) % 4, 1), WZ0 + 4 * pos + 3, at(2, -1))

    def weights_end(xx, pos):
        got(wy(xx, (y + 2) % 4, 0), WY0 + 4 * pos + 2)
        got(wz(xx, (z + 2) % 4, 0), WZ0 + 4 * pos + 2)
        got(wy(xx, (y + 2) % 4, 1), WY0 + 4 * pos + 3)
        got(wz(xx, (z + 2) % 4, 1), WZ0 + 4 * pos + 3)

    left, right, far = (x + 3) % 4, (x + 1) % 4, (x + 2) % 4
    got(wy(left, y), WX0)
    send(wy(left, y, 0), wy(left, y, 0), WX0 + 4, at(0, 1))
    got(wy(right, y), WX0 + 1)
    send(wy(right, y, 1), wy(right, y, 1), WX0 + 5, at(0, -1))
    got(wz(left, z), WX0 + 2)
    send(wz(left, z, 0), wz(left, z, 0), WX0 + 6, at(0, 1))
    got(wz(right, z), WX0 + 3)
    send(wz(right, z, 1), wz(right, z, 1), WX0 + 7, at(0, -1))
    weights_on(left, 0)
    weights_on(right, 1)

    def spread(n, first, base):
        block = jnp.dot(perm[...], gext[pl.ds(first, ROWS), lanes(n, 512)], preferred_element_type=F32)
        for i in range(4):
            ext[n * 4 + i, pl.ds(base, ROWS), :] = block[:, 128 * i : 128 * i + 128]

    loop(4, lambda n: spread(n, 32, ROWS))

    def spread_cot(core):
        def body(n):
            block = jnp.dot(perm[...], cotraw[core, :, lanes(n, 512)], preferred_element_type=F32)
            cotp[rows(core, ROWS), lanes(n, 512)] = block.astype(BF16)

        loop(4, body)

    spread_cot(q)

    @pl.when(s > 0)
    def _():
        got(gext.at[pl.ds(0, 32)], HALO0)

    @pl.when(s == 0)
    def _():
        gext[0:32, :] = jnp.zeros((32, D), BF16)

    loop(4, lambda n: spread(n, 0, 0))

    def got_taps(r):
        src = (s + NSP - 1 - r) % NSP
        got(tkall.at[src], TAP0 + r)

    loop(NSP - 1, got_taps)

    def widen(i):
        tkf[:, lanes(i)] = tkall[i].astype(F32)

    loop(NSP, widen)

    sum1[...] = jnp.zeros((ROWS, 128), F32)
    sum2[...] = jnp.zeros((ROWS, 128), F32)

    def conv_block(i):
        col, jb = i // 4, i % 4
        ln = lanes(col)
        window = {
            o: ext[col, pl.ds(pl.multiple_of((jb * 8 + o + SEG) * 8, 8), 8), :] for o in range(1 - TAPS, 8)
        }
        acc = [None] * 8
        for k in range(TAPS):
            w = jnp.broadcast_to(tkf[k : k + 1, ln], (8, 128))
            for o in range(8):
                term = w * window[o - k]
                acc[o] = term if acc[o] is None else acc[o] + term
        for o in range(8):
            at_rows = pl.ds(pl.multiple_of((jb * 8 + o) * 8, 8), 8)
            cen[col, at_rows, :] = acc[o]
            sum1[at_rows, :] += acc[o]
            sum2[at_rows, :] += acc[o] * acc[o]

    loop(32, conv_block)
    got(wy(far, y, 0), WX0 + 4)
    got(wy(far, y, 1), WX0 + 5)
    got(wz(far, z, 0), WX0 + 6)
    got(wz(far, z, 1), WX0 + 7)
    weights_on(far, 2)
    weights_far(left, 0)
    loop(32, lambda i: conv_block(i + 32))
    weights_far(right, 1)

    mean = jnp.sum(sum1[...], axis=1, keepdims=True) * (1.0 / D)
    var = jnp.sum(sum2[...], axis=1, keepdims=True) * (1.0 / D) - mean * mean
    sum1[...] = jnp.broadcast_to(mean, (ROWS, 128))
    inv_b[...] = jnp.broadcast_to(lax.rsqrt(var + EPS), (ROWS, 128))

    def act_block(i):
        col, jb = i // 4, i % 4
        ln, at_rows = lanes(col), rows(jb, 64)
        centred = (cen[col, at_rows, :] - sum1[at_rows, :]) * inv_b[at_rows, :]
        cen[col, at_rows, :] = centred
        normed = centred * tkf[TAPS : TAPS + 1, ln]
        sg = sigmoid(normed)
        a = normed * sg
        act[pl.ds(pl.multiple_of(q * ROWS + jb * 64, 64), 64), ln] = a.astype(BF16)
        fwd[col, at_rows, :] = sg * (1.0 + normed * (1.0 - sg))

    for g in range(4):
        loop(16, lambda i: act_block(i + 16 * g))
        part = act.at[rows(q, ROWS), pl.ds(512 * g, 512)]
        send(part, part, ACT0 + g, partner)

    weights_far(far, 2)
    got(cotraw.at[1 - q], COT0)
    spread_cot(1 - q)

    blocks = (pa, pb, pc)
    half = lanes(q, HALF)

    def outer(cb):
        p = lax.dot_general(
            act[:, lanes(cb, 256)], cotp[:, half], (((0,), (0,)), ((), ())), preferred_element_type=F32
        ).astype(BF16)
        zz, y0 = cb // 2, (cb % 2) * 2
        for i in range(8):
            yy, xx = y0 + i // 4, i % 4
            piece = p[32 * i : 32 * i + 32]
            pa[xx, yy, zz] = piece[:, 0:384]
            pb[yy, zz, xx] = piece[:, 384:768]
            pc[zz, xx, yy] = piece[:, 768:1024]

    for g in range(4):
        got(act.at[rows(1 - q, ROWS), pl.ds(512 * g, 512)], ACT0 + g)
        loop(2, lambda i: outer(i + 2 * g))

    r1s, cbs = (r1a, r1b, r1c), (cba, cbb, cbc)
    s1s, r2s, s2s, r3s = (s1a, s1b, s1c), (r2a, r2b, r2c), (s2a, s2b, s2c), (r3a, r3b, r3c)
    lo, hi = pl.ds(0, 2), pl.ds(2, 2)
    for c in range(3):
        me = coord[c]
        send(blocks[c].at[(me + 2) % 4, lo], r1s[c].at[0], RA0 + 6 * c, at(c, 1))
        send(blocks[c].at[(me + 2) % 4, hi], r1s[c].at[1], RA0 + 6 * c + 1, at(c, -1))
    for c in range(3):
        me = coord[c]
        send(blocks[c].at[(me + 1) % 4, hi], r1s[c].at[2], RA0 + 6 * c + 2, at(c, 1))
        send(blocks[c].at[(me + 3) % 4, lo], r1s[c].at[3], RA0 + 6 * c + 3, at(c, -1))

    def back_send(pos, xx):
        blk = xx * 2 + q
        g = lax.dot_general(cotp[...], wg[xx], (((1,), (1,)), ((), ())), preferred_element_type=F32).astype(BF16)
        finp[pos] = g
        ga[blk] = finp[pos, rows(q, ROWS), :]
        send(finp.at[pos, rows(1 - q, ROWS)], ga.at[blk], GA0 + pos, partner)

    back_send(3, x)
    weights_end(left, 0)
    back_send(0, left)
    weights_end(right, 1)
    back_send(1, right)
    weights_end(far, 2)
    back_send(2, far)

    def join(c):
        me = coord[c]
        for h, idx, off in ((lo, 0, 1), (hi, 1, -1)):
            got(r1s[c].at[idx], RA0 + 6 * c + idx)
            own = blocks[c].at[(me + off) % 4, h]

            def add(i, own=own, idx=idx):
                a, b = i // 4, i % 4
                total = own[a, b].astype(F32) + r1s[c][idx, a, b].astype(F32)
                cbs[c][idx, a, b] = total.astype(BF16)

            loop(8, add)
            send(cbs[c].at[idx], r1s[c].at[4 + idx], RA0 + 6 * c + 4 + idx, at(c, off))

    for c in range(3):
        join(c)

    for pos, off in ((3, 0), (0, 3), (1, 1), (2, 2)):
        got(ga.at[((x + off) % 4) * 2 + 1 - q], GA0 + pos)

    sum2[...] = jnp.zeros((ROWS, 128), F32)
    halv = sum1
    halv[...] = jnp.zeros((ROWS, 128), F32)

    def grad_block(i):
        ln = lanes(i)
        gain = tkf[TAPS : TAPS + 1, ln]
        gsum = jnp.zeros((8, 128), F32)
        for jb in range(4):
            at_rows = pl.ds(64 * jb, 64)
            up = ga[i // 2, at_rows, lanes(i % 2)].astype(F32)
            gn = up * fwd[i, at_rows, :]
            ce = cen[i, at_rows, :]
            prod = gn * ce
            gsum = gsum + jnp.sum(prod.reshape(8, 8, 128), axis=0)
            gc = gn * gain
            fwd[i, at_rows, :] = gc
            sum1[at_rows, :] += gc
            sum2[at_rows, :] += prod * gain
        gkp[i, TAPS : TAPS + 1, :] = jnp.sum(gsum, axis=0, keepdims=True)

    loop(NSP, grad_block)
    m1 = jnp.sum(sum1[...], axis=1, keepdims=True) * (1.0 / D)
    m2 = jnp.sum(sum2[...], axis=1, keepdims=True) * (1.0 / D)
    sum1[...] = jnp.broadcast_to(m1, (ROWS, 128))
    sum2[...] = jnp.broadcast_to(m2, (ROWS, 128))

    def norm_block(i):
        ln = lanes(i)
        for jb in range(4):
            at_rows = pl.ds(64 * jb, 64)
            fwd[i, at_rows, :] = (
                fwd[i, at_rows, :] - sum1[at_rows, :] - cen[i, at_rows, :] * sum2[at_rows, :]
            ) * inv_b[at_rows, :]
        hal[:, ln] = fwd[i, pl.ds(0, SEG, stride=8), :]

    loop(NSP, norm_block)

    def margin_copy():
        return copy(hal, halr, GC0, {"sp": (s + NSP - 1) % NSP, "dp": d})

    @pl.when(s > 0)
    def _():
        margin_copy().start()

    def tap_block(i):
        col, kb = i // 4, i % 4
        ln = lanes(col)
        acc = [None] * 8
        window = {}
        for j in range(SEG):
            g = fwd[col, pl.ds(8 * j, 8), :]
            for o in range(8):
                if j - o not in window:
                    window[j - o] = ext[col, pl.ds(pl.multiple_of((SEG + j - o - kb * 8) * 8, 8), 8), :]
                term = g * window[j - o]
                acc[o] = term if acc[o] is None else acc[o] + term
        tops = [jnp.sum(a, axis=0, keepdims=True) for a in acc]
        for o in range(7):
            gkp[col, pl.ds(kb * 8 + o, 1), :] = tops[o]

        @pl.when(kb < 3)
        def _():
            gkp[col, pl.ds(kb * 8 + 7, 1), :] = tops[7]

    loop(64, tap_block)

    def send_gk(r):
        dst = (s + r + 1) % NSP
        copy(gkp.at[dst], gkr.at[r], GK0 + r, {"sp": dst, "dp": d}).start()

    loop(NSP - 1, send_gk)

    def stage1(c):
        got(r1s[c].at[2], RA0 + 6 * c + 2)
        got(r1s[c].at[3], RA0 + 6 * c + 3)
        got(r1s[c].at[4], RA0 + 6 * c + 4)
        got(r1s[c].at[5], RA0 + 6 * c + 5)
        me = coord[c]

        def add(i):
            a, b = i // 4, i % 4
            s1s[c][a, b] = (
                blocks[c][me, a, b].astype(F32) + r1s[c][4, a, b].astype(F32) + r1s[c][3, a, b].astype(F32)
            ).astype(BF16)
            s1s[c][a + 2, b] = (
                blocks[c][me, a + 2, b].astype(F32) + r1s[c][2, a, b].astype(F32) + r1s[c][5, a, b].astype(F32)
            ).astype(BF16)

        loop(8, add)
        axis = (c + 1) % 3
        for r in range(1, 4):
            send(s1s[c].at[(coord[axis] + r) % 4], r2s[c].at[r - 1], RB0 + 3 * c + r - 1, at(axis, r))

    def stage2(c):
        axis, last = (c + 1) % 3, (c + 2) % 3
        for r in range(1, 4):
            got(r2s[c].at[r - 1], RB0 + 3 * c + r - 1)

        def add(i):
            total = s1s[c][coord[axis], i].astype(F32)
            for r in range(3):
                total = total + r2s[c][r, i].astype(F32)
            s2s[c][i] = total.astype(BF16)

        loop(4, add)
        for r in range(1, 4):
            send(s2s[c].at[(coord[last] + r) % 4], r3s[c].at[r - 1], RC0 + 3 * c + r - 1, at(last, r))

    factor = float(NSP * NDP * ROWS) ** (-0.5)

    def stage3(c):
        last = (c + 2) % 3
        first, size = COLOURS[c]
        for r in range(1, 4):
            got(r3s[c].at[r - 1], RC0 + 3 * c + r - 1)
        mine = coord[last]
        for to_partner in (False, True):
            h = (1 - q) if to_partner else q
            part = rows(h, 16)
            total = s2s[c][mine, part, :].astype(F32)
            for r in range(3):
                total = total + r3s[c][r, part, :].astype(F32)
            total = total * factor
            if to_partner:
                fins[:, first : first + size] = total
            else:
                ow_ref[:, pl.ds(pl.multiple_of(q * HALF + first, 128), size)] = total

    for c in range(3):
        stage1(c)

    @pl.when(s < NSP - 1)
    def _():
        copy(halr, halr, GC0, partner).wait_recv()

    @pl.when(s == NSP - 1)
    def _():
        halr[...] = jnp.zeros((SEG, D), F32)

    def margin(i):
        ln = lanes(i)
        fwd[i, pl.ds(ROWS, 240), :] = fwd[i, pl.ds(1, 240), :]
        fwd[i, pl.ds(ROWS + 7, SEG, stride=8), :] = halr[:, ln]

    def back_block(i):
        col, jb = i // 4, i % 4
        ln = lanes(col)
        window = {o: fwd[col, pl.ds(pl.multiple_of((jb * 8 + o) * 8, 8), 8), :] for o in range(TAPS + 7)}
        acc = [None] * 8
        for k in range(TAPS):
            w = jnp.broadcast_to(tkf[k : k + 1, ln], (8, 128))
            for o in range(8):
                term = w * window[o + k]
                acc[o] = term if acc[o] is None else acc[o] + term
        for o in range(0, 8, 2):
            at_rows = pl.ds(pl.multiple_of((jb * 8 + o) * 8, 16), 16)
            ggp[at_rows, ln] = jnp.concatenate([acc[o], acc[o + 1]], axis=0).astype(BF16)

    out = []

    def finish(g):
        def body(i):
            cols = lanes(i + 2 * g, 256)
            grad = jnp.dot(permt[...], ggp[:, cols], preferred_element_type=F32)
            sg = sig[:, cols]
            gvo[:, cols] = (grad * sg).astype(BF16)
            ggo[:, cols] = (grad * val[:, cols].astype(F32) * sg * (1.0 - sg)).astype(BF16)

        loop(2, body)
        cols = pl.ds(512 * g, 512)
        for c in (
            pltpu.make_async_copy(gvo.at[:, cols], gv_hbm.at[:, cols], lsem.at[4 + 2 * g]),
            pltpu.make_async_copy(ggo.at[:, cols], gg_hbm.at[:, cols], lsem.at[5 + 2 * g]),
        ):
            c.start()
            out.append(c)

    def group(g):
        loop(4, lambda i: margin(i + 4 * g))
        loop(16, lambda i: back_block(i + 16 * g))
        finish(g)

    group(0)

    def got_gk(r):
        got(gkr.at[r], GK0 + r)

    loop(NSP - 1, got_gk)
    total = gkp[s]
    for r in range(NSP - 1):
        total = total + gkr[r]
    gdo[...] = total

    def send_gd(r):
        copy(gdo, gdr.at[r], GD0 + r, {"sp": s, "dp": (d + r + 1) % NDP}).start()

    loop(NDP - 1, send_gd)
    group(1)
    for c in range(3):
        stage2(c)
    group(2)
    for c in range(3):
        stage3(c)
    send(fins, finr, FIN0, partner)
    group(3)

    def got_gd(r):
        got(gdr.at[r], GD0 + r)

    loop(NDP - 1, got_gd)
    total = gdo[...]
    for r in range(NDP - 1):
        total = total + gdr[r]
    gk_ref[...] = total * factor
    got(finr, FIN0)
    ow_ref[:, lanes(1 - q, HALF)] = finr[...]

    for c in sent:
        c.wait_send()

    def drain_sp(r):
        copy(tkall.at[s], tkall.at[s], TAP0 + r, partner).wait_send()
        copy(gkp.at[s], gkr.at[r], GK0 + r, partner).wait_send()

    loop(NSP - 1, drain_sp)

    def drain_dp(r):
        copy(gdo, gdr.at[r], GD0 + r, partner).wait_send()

    loop(NDP - 1, drain_dp)

    @pl.when(s < NSP - 1)
    def _():
        halo_copy().wait_send()

    @pl.when(s > 0)
    def _():
        margin_copy().wait_send()

    for c in out:
        c.wait()


def shards(out_cotangent, value_pre, gate_pre, out_weight, conv_kernel, norm_gain):
    hbm = pl.BlockSpec(memory_space=pl.ANY)
    vmem = pl.BlockSpec(memory_space=pltpu.VMEM)
    sizes = [size for _, size in COLOURS]
    scratch = [
        ((2, ROWS, D), BF16),
        ((2 * ROWS, D), BF16),
        ((ROWS, D), BF16),
        ((ROWS, D), BF16),
        ((ROWS, D), F32),
        ((ROWS + 32, D), BF16),
        ((NSP, 2 * ROWS, 128), F32),
        ((NSP, ROWS, 128), F32),
        ((NSP, 2 * ROWS, 128), F32),
        ((2 * ROWS, D), BF16),
        ((4, ROWS, D), BF16),
        ((8, ROWS, ROWS), BF16),
        ((32, 128), F32),
        ((NSP, 32, 128), BF16),
        ((32, D), F32),
        ((ROWS, 128), F32),
        ((ROWS, 128), F32),
        ((ROWS, 128), F32),
        ((SEG, D), F32),
        ((SEG, D), F32),
        ((ROWS, D), BF16),
        ((ROWS, D), BF16),
        ((ROWS, D), BF16),
        ((NSP, 32, 128), F32),
        ((NSP - 1, 32, 128), F32),
        ((32, 128), F32),
        ((NDP - 1, 32, 128), F32),
    ]
    scratch += [((4, 4, 4, 32, f), BF16) for f in sizes]
    scratch += [((6, 2, 4, 32, f), BF16) for f in sizes]
    scratch += [((2, 2, 4, 32, f), BF16) for f in sizes]
    scratch += [((4, 4, 32, f), BF16) for f in sizes]
    scratch += [((3, 4, 32, f), BF16) for f in sizes]
    scratch += [((4, 32, f), BF16) for f in sizes]
    scratch += [((3, 32, f), BF16) for f in sizes]
    scratch += [
        ((4, 2 * ROWS, ROWS), BF16),
        ((16, HALF), F32),
        ((16, HALF), F32),
        ((ROWS, ROWS), BF16),
        ((ROWS, ROWS), BF16),
    ]
    grad_value, grad_gate, grad_weight, grad_taps = pl.pallas_call(
        kernel,
        out_shape=(
            jax.ShapeDtypeStruct((ROWS, D), BF16),
            jax.ShapeDtypeStruct((ROWS, D), BF16),
            jax.ShapeDtypeStruct((16, D), F32),
            jax.ShapeDtypeStruct((32, 128), F32),
        ),
        in_specs=[hbm, hbm, hbm, hbm, vmem, vmem],
        out_specs=(hbm, hbm, vmem, vmem),
        scratch_shapes=[pltpu.VMEM(shape, kind) for shape, kind in scratch]
        + [pltpu.SemaphoreType.DMA((NSEM,)), pltpu.SemaphoreType.DMA((NSEM,)), pltpu.SemaphoreType.DMA((12,))],
        compiler_params=pltpu.CompilerParams(
            collective_id=0, has_side_effects=True, vmem_limit_bytes=60 * 1024 * 1024
        ),
    )(out_cotangent[0], value_pre[0], gate_pre[0], out_weight, conv_kernel, norm_gain[None])
    return (grad_value[None], grad_gate[None], grad_weight, grad_taps[:TAPS], grad_taps[TAPS])


def solution(mesh):
    placed = (
        P("dp", "sp", None),
        P("dp", "sp", None),
        P("dp", "sp", None),
        P("dp", None),
        P(None, "sp"),
        P("sp"),
    )
    return jax.shard_map(
        shards,
        mesh=mesh,
        in_specs=placed,
        out_specs=(
            P("dp", "sp", None),
            P("dp", "sp", None),
            P(("sp", "dp"), None),
            P(None, "sp"),
            P("sp"),
        ),
        check_vma=False,
    )
```

time: 172 us -> 78.3 us (0.46)
  Pallas kernels: 0 us -> 70.8 us
  other arithmetic: 51.2 us -> 0 us
  starting transfers between devices: 31 us -> 0 us
  waiting for transfers between devices: 25.9 us -> 0 us
  blocking collectives: 20.8 us -> 0 us
  between operations: 15.9 us -> 0.65 us
  matrix products: 15.2 us -> 0 us
  local copies, waits for them, and re-layouts: 10.3 us -> 5.94 us
    pallas_call x0 -> x1, Pallas kernels: none -> 70.8 us  [shards(): pl.pallas_call(kernel, out_shape=(jax.ShapeDtypeStruct((ROWS, D), BF16),...]
    reduce_sum x7 -> x0, other arithmetic: 26 us -> none  [the longest x2 12.9 us: mechanism(): jnp.sum(grad_conv * extended[begin:begin + row_count], axis=0)]
    all_to_all x4 -> x0, starting transfers between devices: 25.6 us -> none  [the longest x2 13.3 us: summed_on_arrival(): blocks = lax.all_to_all(cut_along(x, dim, devices), axis, 0, 0, tiled=True)]
    all_gather x1 -> x0, blocking collectives: 20.8 us -> none  [rows_first(): whole, at, outs = (lax.all_gather(both, axis, axis=0, tiled=True), 0, [])]
    broadcast_in_dim x2 -> x0, other arithmetic: 19.5 us -> none  [the longest x1 16.4 us: shards(): grad_gates[None]]
    dot_general x2 -> x0, matrix products: 15.2 us -> none  [the longest x1 9.14 us: shards(): lax.dot_general(cotangent, lax.all_gather(out_weight, 'dp', axis=0, tiled...]
    all_to_all x4 -> x0, waiting for transfers between devices: 10.9 us -> none  [the longest x2 5.9 us: summed_on_arrival(): blocks = lax.all_to_all(cut_along(x, dim, devices), axis, 0, 0, tiled=True)]
    all_gather x1 -> x0, waiting for transfers between devices: 8.64 us -> none  [shards(): lax.all_gather(out_weight, 'dp', axis=0, tiled=True)]
  transfers between devices with their start and end apart: 8 -> 0, of which waited for: 4 -> 0; matrix products, arithmetic and copies ran while one was open for 44% -> 0% of each run, Pallas kernels for 0% -> 0%
where the time goes in v1:
time: 78.3 us; the launch traced here: 77.4 us
  Pallas kernels  70.8 us (90%)
  local copies, waits for them, and re-layouts  5.94 us (8%)
    pallas_call x1, Pallas kernels, shards(): pl.pallas_call(kernel, out_shape=(jax.ShapeDtypeStruct((ROWS, D), BF16),...  70.8 us
    unnamed x10, local copies, waits for them, and re-layouts  4.74 us

profile of v1, /device:TPU:1, one launch (start us, length us, event | category | flops | bytes accessed | tf_op | source)
XLA Modules:
  0.0 77.4 jit_solution(16990111440105515977)
XLA Ops:
  0.6 70.8 %shard_map.101 = (bf16[256,2048]{1,0:T(8,128)(2,1)}, bf16[256,2048]{1,0:T(8,128)(2,1)}, f32[16,2048]{1,0:T(8,128)}, f32[32,128]{1,0:T(8,128)}) custom-call(bf16[256,2048]{1,0:T(8,128)(2,1)} %bitcast.9, bf16[256,2048]{1,0:T(8,128)(2,1)} %bitcast.10, bf16[256,2048]{1,0:T(8,128)(2,1)} %bitcast.11, bf16[256,2048]{1,0:T(8,128)(2,1)} %w_hbm.1, ...), custom_call_target="tpu_custom_call" | custom-call | tf_op jit(solution)/shard_map/pallas_call | solution.py:712
  71.4 1.2 %slice_bitcast_fusion = f32[128]{0:T(128)} fusion(f32[32,128]{1,0:T(8,128)} %get-tuple-element.12), kind=kLoop, calls=%fused_computation | loop fusion | bytes 1024 | tf_op jit(solution)/shard_map/squeeze | solution.py:728
  72.6 0.0 copy-start
  72.6 2.4 %copy.15 = bf16[1,256,2048]{2,1,0:T(8,128)(2,1)} copy(bf16[1,256,2048]{2,1,0:T(8,128)(2,1)} %bitcast.13) | data formatting | bytes 2097152
  75.0 0.0 copy-done
  75.0 0.0 copy-start.1
  75.0 1.0 %copy.16 = bf16[1,256,2048]{2,1,0:T(8,128)(2,1)} copy(bf16[1,256,2048]{2,1,0:T(8,128)(2,1)S(1)} %bitcast.12) | data formatting | bytes 2097152
  76.0 0.1 copy-done.1
  76.1 0.0 copy-start.2
  76.1 0.7 copy.17
  76.7 0.1 copy-done.2
  76.8 0.6 copy.18
Async XLA Ops:
  72.6 2.4 %copy-start = (bf16[256,2048]{1,0:T(8,128)(2,1)S(1)}, bf16[256,2048]{1,0:T(8,128)(2,1)}, u32[]{:S(2)}) copy-start(bf16[256,2048]{1,0:T(8,128)(2,1)} %get-tuple-element.10) | copy-start | bytes 3145732
  75.0 1.0 %copy-start.1 = (f32[16,2048]{1,0:T(8,128)S(1)}, f32[16,2048]{1,0:T(8,128)}, u32[]{:S(2)}) copy-start(f32[16,2048]{1,0:T(8,128)} %get-tuple-element.20) | copy-start | bytes 393220
  76.1 0.7 copy-start.2

commit v2 on v1

--- a/solution.py
+++ b/solution.py
@@ -13,19 +13,20 @@
 MESH = pl.DeviceIdType.MESH
 
 ROWS = 256
-SEG = 32
+SEG = 16
 D = 2048
 HALF = 1024
 TAPS = 31
 NSP = 16
 NDP = 8
+WX_COLS, WY_COLS, WZ_COLS = (0, 512), (512, 768), (1280, 768)
 COLOURS = ((0, 384), (384, 384), (768, 256))
 
 TAP0 = 0
 COT0 = TAP0 + 16
 HALO0 = COT0 + 1
 WX0 = HALO0 + 1
-WY0 = WX0 + 8
+WY0 = WX0 + 12
 WZ0 = WY0 + 12
 ACT0 = WZ0 + 12
 GA0 = ACT0 + 4
@@ -84,12 +85,14 @@
     ga,
     tkown,
     tkall,
-    tkf,
+    taps,
+    gains,
     sum1,
     sum2,
     inv_b,
-    hal,
-    halr,
+    later,
+    gcp,
+    gcraw,
     ggp,
     gvo,
     ggo,
@@ -122,7 +125,6 @@
     fins,
     finr,
     perm,
-    permt,
     ssem,
     rsem,
     lsem,
@@ -180,23 +182,22 @@
     tkall[s] = tkown[...].astype(BF16)
     r_io = lax.broadcasted_iota(jnp.int32, (ROWS, ROWS), 0)
     t_io = lax.broadcasted_iota(jnp.int32, (ROWS, ROWS), 1)
-    perm[...] = jnp.where(t_io == (r_io & 7) * SEG + (r_io >> 3), 1.0, 0.0).astype(BF16)
-    permt[...] = jnp.where(r_io == (t_io & 7) * SEG + (t_io >> 3), 1.0, 0.0).astype(BF16)
+    perm[...] = jnp.where(t_io == (r_io & 15) * SEG + (r_io >> 4), 1.0, 0.0).astype(BF16)
     pl.semaphore_wait(barrier, NSP - 1 + NDP - 1)
 
-    def wy(xx, yy, h=None):
-        if h is None:
-            return wg.at[xx, pl.ds(pl.multiple_of(yy * 64, 64), 64), pl.ds(0, HALF)]
-        return wg.at[xx, pl.ds(pl.multiple_of(yy * 64 + h * 32, 32), 32), pl.ds(0, HALF)]
-
-    def wz(xx, zz, h=None):
-        if h is None:
-            return wg.at[xx, pl.ds(pl.multiple_of(zz * 64, 64), 64), pl.ds(HALF, HALF)]
-        return wg.at[xx, pl.ds(pl.multiple_of(zz * 64 + h * 32, 32), 32), pl.ds(HALF, HALF)]
+    def piece(cols, size):
+        def at_quarter(xx, quarter, h=None):
+            n, first = (size, quarter * size) if h is None else (size // 2, quarter * size + h * (size // 2))
+            return wg.at[xx, pl.ds(pl.multiple_of(first, n), n), pl.ds(*cols)]
+
+        return at_quarter
+
+    wx, wy, wz = piece(WX_COLS, ROWS), piece(WY_COLS, 64), piece(WZ_COLS, 64)
 
     local[0].wait()
     for i, off in ((0, 1), (1, -1)):
         send(wy(x, y), wy(x, y), WX0 + i, at(0, off))
+    for i, off in ((0, 1), (1, -1)):
         send(wz(x, z), wz(x, z), WX0 + 2 + i, at(0, off))
 
     def send_taps(r):
@@ -226,54 +227,94 @@
     send(cotraw.at[q], cotraw.at[q], COT0, partner)
     loop(ROWS // 32 - 1, lambda i: gate_block(i + 1))
 
-    def weights_on(xx, pos):
-        for i, off in ((0, 1), (1, -1)):
-            send(wy(xx, y), wy(xx, y), WY0 + 4 * pos + i, at(1, off))
-            send(wz(xx, z), wz(xx, z), WZ0 + 4 * pos + i, at(2, off))
-
-    def weights_far(xx, pos):
-        got(wy(xx, (y + 3) % 4), WY0 + 4 * pos)
-        send(wy(xx, (y + 3) % 4, 0), wy(xx, (y + 3) % 4, 0), WY0 + 4 * pos + 2, at(1, 1))
-        got(wz(xx, (z + 3) % 4), WZ0 + 4 * pos)
-        send(wz(xx, (z + 3) % 4, 0), wz(xx, (z + 3) % 4, 0), WZ0 + 4 * pos + 2, at(2, 1))
-        got(wy(xx, (y + 1) % 4), WY0 + 4 * pos + 1)
-        send(wy(xx, (y + 1) % 4, 1), wy(xx, (y + 1) % 4, 1), WY0 + 4 * pos + 3, at(1, -1))
-        got(wz(xx, (z + 1) % 4), WZ0 + 4 * pos + 1)
-        send(wz(xx, (z + 1) % 4, 1), wz(xx, (z + 1) % 4, 1), WZ0 + 4 * pos + 3, at(2, -1))
+    left, right, far = (x + 3) % 4, (x + 1) % 4, (x + 2) % 4
+    both = ((0, 1), (1, -1))
+
+    def along_x(part, quarter, base):
+        for i, off in both:
+            src = (x - off) % 4
+            got(part(src, quarter), WX0 + base + i)
+            send(part(src, quarter, i), part(src, quarter, i), WX0 + 6 + base + i, at(0, off))
+
+    def far_along_x(part, quarter, base):
+        for i, _ in both:
+            got(part(far, quarter, i), WX0 + 6 + base + i)
+
+    def across(axis, xx, pos):
+        part, here, base = ((wy, y, WY0), (wz, z, WZ0))[axis - 1]
+        for i, off in both:
+            send(part(xx, here), part(xx, here), base + 4 * pos + i, at(axis, off))
+
+    def across_on(axis, xx, pos):
+        part, here, base = ((wy, y, WY0), (wz, z, WZ0))[axis - 1]
+        for i, off in both:
+            quarter = (here - off) % 4
+            got(part(xx, quarter), base + 4 * pos + i)
+            send(part(xx, quarter, i), part(xx, quarter, i), base + 4 * pos + 2 + i, at(axis, off))
+
+    def across_end(axis, xx, pos):
+        part, here, base = ((wy, y, WY0), (wz, z, WZ0))[axis - 1]
+        for i, _ in both:
+            got(part(xx, (here + 2) % 4, i), base + 4 * pos + 2 + i)
+
+    def weights1():
+        along_x(wy, y, 0)
+        across(1, left, 0)
+        across(1, right, 1)
+
+    def weights2():
+        along_x(wz, z, 2)
+        across(2, left, 0)
+        across(2, right, 1)
+        for i, off in both:
+            send(wx(x, 0), wx(x, 0), WX0 + 4 + i, at(0, off))
+
+    def weights3():
+        far_along_x(wy, y, 0)
+        across(1, far, 2)
+        across_on(1, left, 0)
+
+    def weights4():
+        far_along_x(wz, z, 2)
+        across(2, far, 2)
+        across_on(1, right, 1)
+        across_on(2, left, 0)
+
+    def weights5():
+        across_on(2, right, 1)
+        across_on(1, far, 2)
+        along_x(wx, 0, 4)
+
+    def weights6():
+        across_on(2, far, 2)
 
     def weights_end(xx, pos):
-        got(wy(xx, (y + 2) % 4, 0), WY0 + 4 * pos + 2)
-        got(wz(xx, (z + 2) % 4, 0), WZ0 + 4 * pos + 2)
-        got(wy(xx, (y + 2) % 4, 1), WY0 + 4 * pos + 3)
-        got(wz(xx, (z + 2) % 4, 1), WZ0 + 4 * pos + 3)
-
-    left, right, far = (x + 3) % 4, (x + 1) % 4, (x + 2) % 4
-    got(wy(left, y), WX0)
-    send(wy(left, y, 0), wy(left, y, 0), WX0 + 4, at(0, 1))
-    got(wy(right, y), WX0 + 1)
-    send(wy(right, y, 1), wy(right, y, 1), WX0 + 5, at(0, -1))
-    got(wz(left, z), WX0 + 2)
-    send(wz(left, z, 0), wz(left, z, 0), WX0 + 6, at(0, 1))
-    got(wz(right, z), WX0 + 3)
-    send(wz(right, z, 1), wz(right, z, 1), WX0 + 7, at(0, -1))
-    weights_on(left, 0)
-    weights_on(right, 1)
-
-    def spread(n, first, base):
-        block = jnp.dot(perm[...], gext[pl.ds(first, ROWS), lanes(n, 512)], preferred_element_type=F32)
-        for i in range(4):
-            ext[n * 4 + i, pl.ds(base, ROWS), :] = block[:, 128 * i : 128 * i + 128]
-
-    loop(4, lambda n: spread(n, 32, ROWS))
+        across_end(1, xx, pos)
+        across_end(2, xx, pos)
+        if pos == 2:
+            far_along_x(wx, 0, 4)
+
+    def spread(src, first, dst, base):
+        def body(n):
+            block = jnp.dot(perm[...], src[pl.ds(first, ROWS), lanes(n, 1024)], preferred_element_type=F32)
+            block = block.astype(BF16)
+            for i in range(8):
+                dst[n * 8 + i, pl.ds(base, ROWS), :] = block[:, 128 * i : 128 * i + 128]
+
+        loop(2, body)
+
+    spread(gext, 32, ext, 2 * ROWS)
 
     def spread_cot(core):
         def body(n):
-            block = jnp.dot(perm[...], cotraw[core, :, lanes(n, 512)], preferred_element_type=F32)
-            cotp[rows(core, ROWS), lanes(n, 512)] = block.astype(BF16)
-
-        loop(4, body)
+            block = jnp.dot(perm[...], cotraw[core, :, lanes(n, 1024)], preferred_element_type=F32)
+            cotp[rows(core, ROWS), lanes(n, 1024)] = block.astype(BF16)
+
+        loop(2, body)
 
     spread_cot(q)
+    got(cotraw.at[1 - q], COT0)
+    spread_cot(1 - q)
 
     @pl.when(s > 0)
     def _():
@@ -283,7 +324,9 @@
     def _():
         gext[0:32, :] = jnp.zeros((32, D), BF16)
 
-    loop(4, lambda n: spread(n, 0, 0))
+    weights1()
+    spread(gext, 16, ext, ROWS)
+    spread(gext, 0, ext, 0)
 
     def got_taps(r):
         src = (s + NSP - 1 - r) % NSP
@@ -292,65 +335,73 @@
     loop(NSP - 1, got_taps)
 
     def widen(i):
-        tkf[:, lanes(i)] = tkall[i].astype(F32)
+        t = tkall[i].astype(F32)
+        gains[:, lanes(i)] = jnp.broadcast_to(t[TAPS : TAPS + 1], (16, 128))
+        for k in range(TAPS):
+            taps[i, 16 * k : 16 * k + 16, :] = jnp.broadcast_to(t[k : k + 1], (16, 128)).astype(BF16)
 
     loop(NSP, widen)
 
-    sum1[...] = jnp.zeros((ROWS, 128), F32)
-    sum2[...] = jnp.zeros((ROWS, 128), F32)
-
-    def conv_block(i):
-        col, jb = i // 4, i % 4
-        ln = lanes(col)
-        window = {
-            o: ext[col, pl.ds(pl.multiple_of((jb * 8 + o + SEG) * 8, 8), 8), :] for o in range(1 - TAPS, 8)
-        }
-        acc = [None] * 8
-        for k in range(TAPS):
-            w = jnp.broadcast_to(tkf[k : k + 1, ln], (8, 128))
-            for o in range(8):
-                term = w * window[o - k]
-                acc[o] = term if acc[o] is None else acc[o] + term
-        for o in range(8):
-            at_rows = pl.ds(pl.multiple_of((jb * 8 + o) * 8, 8), 8)
-            cen[col, at_rows, :] = acc[o]
-            sum1[at_rows, :] += acc[o]
-            sum2[at_rows, :] += acc[o] * acc[o]
-
-    loop(32, conv_block)
-    got(wy(far, y, 0), WX0 + 4)
-    got(wy(far, y, 1), WX0 + 5)
-    got(wz(far, z, 0), WX0 + 6)
-    got(wz(far, z, 1), WX0 + 7)
-    weights_on(far, 2)
-    weights_far(left, 0)
-    loop(32, lambda i: conv_block(i + 32))
-    weights_far(right, 1)
-
+    def filtered(col, src, shift, emit):
+        tiles, weights = src.at[col], taps.at[col]
+        for j0 in range(0, SEG, 4):
+            acc = [None] * 4
+            for k in range(TAPS):
+                for o in range(4):
+                    at_row = 16 * shift(j0 + o, k)
+                    term = weights[16 * k : 16 * k + 16, :].astype(F32) * tiles[at_row : at_row + 16, :].astype(F32)
+                    acc[o] = term if acc[o] is None else acc[o] + term
+            for o in range(4):
+                emit(j0 + o, acc[o])
+
+    def conv_block(col):
+        dst = cen.at[col]
+
+        def emit(j, v):
+            dst[16 * j : 16 * j + 16, :] = v
+
+        filtered(col, ext, lambda j, k: j - k + 2 * SEG, emit)
+
+    loop(NSP, conv_block)
+
+    weights2()
+
+    def conv_sums(j):
+        at_rows = rows(j, 16)
+        one = two = None
+        for col in range(NSP):
+            v = cen[col, at_rows, :]
+            one = v if one is None else one + v
+            two = v * v if two is None else two + v * v
+        sum1[at_rows, :] = one
+        sum2[at_rows, :] = two
+
+    loop(SEG, conv_sums)
     mean = jnp.sum(sum1[...], axis=1, keepdims=True) * (1.0 / D)
     var = jnp.sum(sum2[...], axis=1, keepdims=True) * (1.0 / D) - mean * mean
     sum1[...] = jnp.broadcast_to(mean, (ROWS, 128))
     inv_b[...] = jnp.broadcast_to(lax.rsqrt(var + EPS), (ROWS, 128))
 
-    def act_block(i):
-        col, jb = i // 4, i % 4
-        ln, at_rows = lanes(col), rows(jb, 64)
-        centred = (cen[col, at_rows, :] - sum1[at_rows, :]) * inv_b[at_rows, :]
-        cen[col, at_rows, :] = centred
-        normed = centred * tkf[TAPS : TAPS + 1, ln]
-        sg = sigmoid(normed)
-        a = normed * sg
-        act[pl.ds(pl.multiple_of(q * ROWS + jb * 64, 64), 64), ln] = a.astype(BF16)
-        fwd[col, at_rows, :] = sg * (1.0 + normed * (1.0 - sg))
+    def act_block(g, j):
+        at_rows = rows(j, 16)
+        m, iv = sum1[at_rows, :], inv_b[at_rows, :]
+        for col in range(4 * g, 4 * g + 4):
+            ln = pl.ds(128 * col, 128)
+            centred = (cen[col, at_rows, :] - m) * iv
+            cen[col, at_rows, :] = centred
+            normed = centred * gains[:, ln]
+            sg = sigmoid(normed)
+            act[pl.ds(pl.multiple_of(q * ROWS + j * 16, 16), 16), ln] = (normed * sg).astype(BF16)
+            fwd[col, at_rows, :] = sg * (1.0 + normed * (1.0 - sg))
 
     for g in range(4):
-        loop(16, lambda i: act_block(i + 16 * g))
+        loop(SEG, lambda j: act_block(g, j))
         part = act.at[rows(q, ROWS), pl.ds(512 * g, 512)]
         send(part, part, ACT0 + g, partner)
-
-    weights_far(far, 2)
-    got(cotraw.at[1 - q], COT0)
-    spread_cot(1 - q)
+        if g == 1:
+            weights3()
+
+    weights4()
 
     blocks = (pa, pb, pc)
     half = lanes(q, HALF)
@@ -370,10 +421,13 @@
     for g in range(4):
         got(act.at[rows(1 - q, ROWS), pl.ds(512 * g, 512)], ACT0 + g)
         loop(2, lambda i: outer(i + 2 * g))
+        if g == 1:
+            weights5()
 
     r1s, cbs = (r1a, r1b, r1c), (cba, cbb, cbc)
     s1s, r2s, s2s, r3s = (s1a, s1b, s1c), (r2a, r2b, r2c), (s2a, s2b, s2c), (r3a, r3b, r3c)
     lo, hi = pl.ds(0, 2), pl.ds(2, 2)
+    weights6()
     for c in range(3):
         me = coord[c]
         send(blocks[c].at[(me + 2) % 4, lo], r1s[c].at[0], RA0 + 6 * c, at(c, 1))
@@ -418,72 +472,72 @@
     for pos, off in ((3, 0), (0, 3), (1, 1), (2, 2)):
         got(ga.at[((x + off) % 4) * 2 + 1 - q], GA0 + pos)
 
-    sum2[...] = jnp.zeros((ROWS, 128), F32)
-    halv = sum1
-    halv[...] = jnp.zeros((ROWS, 128), F32)
-
-    def grad_block(i):
-        ln = lanes(i)
-        gain = tkf[TAPS : TAPS + 1, ln]
-        gsum = jnp.zeros((8, 128), F32)
-        for jb in range(4):
-            at_rows = pl.ds(64 * jb, 64)
-            up = ga[i // 2, at_rows, lanes(i % 2)].astype(F32)
-            gn = up * fwd[i, at_rows, :]
-            ce = cen[i, at_rows, :]
-            prod = gn * ce
-            gsum = gsum + jnp.sum(prod.reshape(8, 8, 128), axis=0)
+    def grad_block(j, gsums):
+        at_rows = rows(j, 16)
+        one = two = None
+        out_sums = []
+        for col in range(NSP):
+            ln = pl.ds(128 * col, 128)
+            gn = ga[col // 2, at_rows, pl.ds(128 * (col % 2), 128)].astype(F32) * fwd[col, at_rows, :]
+            prod = gn * cen[col, at_rows, :]
+            out_sums.append(gsums[col] + prod[0:8] + prod[8:16])
+            gain = gains[:, ln]
             gc = gn * gain
-            fwd[i, at_rows, :] = gc
-            sum1[at_rows, :] += gc
-            sum2[at_rows, :] += prod * gain
-        gkp[i, TAPS : TAPS + 1, :] = jnp.sum(gsum, axis=0, keepdims=True)
-
-    loop(NSP, grad_block)
+            fwd[col, at_rows, :] = gc
+            prod = prod * gain
+            one = gc if one is None else one + gc
+            two = prod if two is None else two + prod
+        sum1[at_rows, :] = one
+        sum2[at_rows, :] = two
+        return out_sums
+
+    gsums = lax.fori_loop(0, SEG, grad_block, [jnp.zeros((8, 128), F32)] * NSP)
+    for col in range(NSP):
+        gkp[col, TAPS : TAPS + 1, :] = jnp.sum(gsums[col], axis=0, keepdims=True)
     m1 = jnp.sum(sum1[...], axis=1, keepdims=True) * (1.0 / D)
     m2 = jnp.sum(sum2[...], axis=1, keepdims=True) * (1.0 / D)
     sum1[...] = jnp.broadcast_to(m1, (ROWS, 128))
     sum2[...] = jnp.broadcast_to(m2, (ROWS, 128))
 
-    def norm_block(i):
-        ln = lanes(i)
-        for jb in range(4):
-            at_rows = pl.ds(64 * jb, 64)
-            fwd[i, at_rows, :] = (
-                fwd[i, at_rows, :] - sum1[at_rows, :] - cen[i, at_rows, :] * sum2[at_rows, :]
-            ) * inv_b[at_rows, :]
-        hal[:, ln] = fwd[i, pl.ds(0, SEG, stride=8), :]
-
-    loop(NSP, norm_block)
+    def norm_block(j):
+        at_rows = rows(j, 16)
+        a, b, iv = sum1[at_rows, :], sum2[at_rows, :], inv_b[at_rows, :]
+        for col in range(NSP):
+            v = ((fwd[col, at_rows, :] - a - cen[col, at_rows, :] * b) * iv).astype(BF16)
+            later[col, at_rows, :] = v
+            gcp[at_rows, pl.ds(128 * col, 128)] = v
+
+    loop(SEG, norm_block)
+
+    def in_order(n):
+        block = jnp.dot(perm[...], gcp[:, lanes(n, 1024)], preferred_element_type=F32)
+        gcraw[0:ROWS, lanes(n, 1024)] = block.astype(BF16)
+
+    loop(2, in_order)
 
     def margin_copy():
-        return copy(hal, halr, GC0, {"sp": (s + NSP - 1) % NSP, "dp": d})
+        return copy(
+            gcraw.at[pl.ds(0, 32)], gcraw.at[pl.ds(ROWS, 32)], GC0, {"sp": (s + NSP - 1) % NSP, "dp": d}
+        )
 
     @pl.when(s > 0)
     def _():
         margin_copy().start()
 
-    def tap_block(i):
-        col, kb = i // 4, i % 4
-        ln = lanes(col)
-        acc = [None] * 8
-        window = {}
-        for j in range(SEG):
-            g = fwd[col, pl.ds(8 * j, 8), :]
-            for o in range(8):
-                if j - o not in window:
-                    window[j - o] = ext[col, pl.ds(pl.multiple_of((SEG + j - o - kb * 8) * 8, 8), 8), :]
-                term = g * window[j - o]
-                acc[o] = term if acc[o] is None else acc[o] + term
-        tops = [jnp.sum(a, axis=0, keepdims=True) for a in acc]
-        for o in range(7):
-            gkp[col, pl.ds(kb * 8 + o, 1), :] = tops[o]
-
-        @pl.when(kb < 3)
-        def _():
-            gkp[col, pl.ds(kb * 8 + 7, 1), :] = tops[7]
-
-    loop(64, tap_block)
+    def tap_block(col):
+        grads, tiles, sums = later.at[col], ext.at[col], gkp.at[col]
+        for k0 in range(0, TAPS, 4):
+            taps_here = range(k0, min(k0 + 4, TAPS))
+            acc = {}
+            for j in range(SEG):
+                for k in taps_here:
+                    at_row = 16 * (j - k + 2 * SEG)
+                    term = grads[16 * j : 16 * j + 16, :].astype(F32) * tiles[at_row : at_row + 16, :].astype(F32)
+                    acc[k] = term if j == 0 else acc[k] + term
+            for k in taps_here:
+                sums[k : k + 1, :] = jnp.sum(acc[k][0:8] + acc[k][8:16], axis=0, keepdims=True)
+
+    loop(NSP, tap_block)
 
     def send_gk(r):
         dst = (s + r + 1) % NSP
@@ -552,43 +606,31 @@
 
     @pl.when(s < NSP - 1)
     def _():
-        copy(halr, halr, GC0, partner).wait_recv()
+        got(gcraw.at[pl.ds(ROWS, 32)], GC0)
 
     @pl.when(s == NSP - 1)
     def _():
-        halr[...] = jnp.zeros((SEG, D), F32)
-
-    def margin(i):
-        ln = lanes(i)
-        fwd[i, pl.ds(ROWS, 240), :] = fwd[i, pl.ds(1, 240), :]
-        fwd[i, pl.ds(ROWS + 7, SEG, stride=8), :] = halr[:, ln]
-
-    def back_block(i):
-        col, jb = i // 4, i % 4
+        gcraw[ROWS : ROWS + 32, :] = jnp.zeros((32, D), BF16)
+
+    spread(gcraw, 16, later, ROWS)
+    spread(gcraw, 32, later, 2 * ROWS)
+
+    def back_block(col):
         ln = lanes(col)
-        window = {o: fwd[col, pl.ds(pl.multiple_of((jb * 8 + o) * 8, 8), 8), :] for o in range(TAPS + 7)}
-        acc = [None] * 8
-        for k in range(TAPS):
-            w = jnp.broadcast_to(tkf[k : k + 1, ln], (8, 128))
-            for o in range(8):
-                term = w * window[o + k]
-                acc[o] = term if acc[o] is None else acc[o] + term
-        for o in range(0, 8, 2):
-            at_rows = pl.ds(pl.multiple_of((jb * 8 + o) * 8, 16), 16)
-            ggp[at_rows, ln] = jnp.concatenate([acc[o], acc[o + 1]], axis=0).astype(BF16)
+
+        def emit(j, v):
+            ggp[16 * j : 16 * j + 16, ln] = v.astype(BF16)
+
+        filtered(col, later, lambda j, k: j + k, emit)
 
     out = []
 
     def finish(g):
-        def body(i):
-            cols = lanes(i + 2 * g, 256)
-            grad = jnp.dot(permt[...], ggp[:, cols], preferred_element_type=F32)
-            sg = sig[:, cols]
-            gvo[:, cols] = (grad * sg).astype(BF16)
-            ggo[:, cols] = (grad * val[:, cols].astype(F32) * sg * (1.0 - sg)).astype(BF16)
-
-        loop(2, body)
         cols = pl.ds(512 * g, 512)
+        grad = jnp.dot(perm[...], ggp[:, cols], preferred_element_type=F32)
+        sg = sig[:, cols]
+        gvo[:, cols] = (grad * sg).astype(BF16)
+        ggo[:, cols] = (grad * val[:, cols].astype(F32) * sg * (1.0 - sg)).astype(BF16)
         for c in (
             pltpu.make_async_copy(gvo.at[:, cols], gv_hbm.at[:, cols], lsem.at[4 + 2 * g]),
             pltpu.make_async_copy(ggo.at[:, cols], gg_hbm.at[:, cols], lsem.at[5 + 2 * g]),
@@ -597,8 +639,7 @@
             out.append(c)
 
     def group(g):
-        loop(4, lambda i: margin(i + 4 * g))
-        loop(16, lambda i: back_block(i + 16 * g))
+        loop(4, lambda i: back_block(i + 4 * g))
         finish(g)
 
     group(0)
@@ -660,6 +701,34 @@
 
     for c in out:
         c.wait()
+
+
+def place(gv_in, gg_in, ow_in, gk_in, gv_hbm, gg_hbm, ow_hbm, taps_hbm, gain_hbm, gv, gg, ow, gk, tp, gn, lsem, ssem):
+    ins, outs = [], []
+    for i in range(4):
+        at_rows = pl.ds(64 * i, 64)
+        ins.append(pltpu.make_async_copy(gv_in.at[at_rows], gv.at[at_rows], lsem.at[2 * i]))
+        outs.append(pltpu.make_async_copy(gv.at[at_rows], gv_hbm.at[at_rows], ssem.at[2 * i]))
+        ins.append(pltpu.make_async_copy(gg_in.at[at_rows], gg.at[at_rows], lsem.at[2 * i + 1]))
+        outs.append(pltpu.make_async_copy(gg.at[at_rows], gg_hbm.at[at_rows], ssem.at[2 * i + 1]))
+    ins.append(pltpu.make_async_copy(ow_in, ow, lsem.at[8]))
+    outs.append(pltpu.make_async_copy(ow, ow_hbm, ssem.at[8]))
+    small = pltpu.make_async_copy(gk_in, gk, lsem.at[9])
+    small.start()
+    for c in ins:
+        c.start()
+    for c, o in zip(ins, outs):
+        c.wait()
+        o.start()
+    small.wait()
+    tp[...] = gk[0:TAPS, :]
+    gn[...] = gk[TAPS : TAPS + 1, :]
+    outs.append(pltpu.make_async_copy(tp, taps_hbm, ssem.at[9]))
+    outs.append(pltpu.make_async_copy(gn, gain_hbm, ssem.at[10]))
+    outs[-2].start()
+    outs[-1].start()
+    for o in outs:
+        o.wait()
 
 
 def shards(out_cotangent, value_pre, gate_pre, out_weight, conv_kernel, norm_gain):
@@ -673,20 +742,22 @@
         ((ROWS, D), BF16),
         ((ROWS, D), F32),
         ((ROWS + 32, D), BF16),
-        ((NSP, 2 * ROWS, 128), F32),
+        ((NSP, 3 * ROWS, 128), BF16),
         ((NSP, ROWS, 128), F32),
-        ((NSP, 2 * ROWS, 128), F32),
+        ((NSP, ROWS, 128), F32),
         ((2 * ROWS, D), BF16),
         ((4, ROWS, D), BF16),
         ((8, ROWS, ROWS), BF16),
         ((32, 128), F32),
         ((NSP, 32, 128), BF16),
-        ((32, D), F32),
+        ((NSP, 16 * TAPS, 128), BF16),
+        ((16, D), F32),
         ((ROWS, 128), F32),
         ((ROWS, 128), F32),
         ((ROWS, 128), F32),
-        ((SEG, D), F32),
-        ((SEG, D), F32),
+        ((NSP, 3 * ROWS, 128), BF16),
+        ((ROWS, D), BF16),
+        ((ROWS + 32, D), BF16),
         ((ROWS, D), BF16),
         ((ROWS, D), BF16),
         ((ROWS, D), BF16),
@@ -707,7 +778,6 @@
         ((16, HALF), F32),
         ((16, HALF), F32),
         ((ROWS, ROWS), BF16),
-        ((ROWS, ROWS), BF16),
     ]
     grad_value, grad_gate, grad_weight, grad_taps = pl.pallas_call(
         kernel,
@@ -725,7 +795,29 @@
             collective_id=0, has_side_effects=True, vmem_limit_bytes=60 * 1024 * 1024
         ),
     )(out_cotangent[0], value_pre[0], gate_pre[0], out_weight, conv_kernel, norm_gain[None])
-    return (grad_value[None], grad_gate[None], grad_weight, grad_taps[:TAPS], grad_taps[TAPS])
+    grad_value, grad_gate, grad_weight, grad_kernel, grad_gain = pl.pallas_call(
+        place,
+        out_shape=(
+            jax.ShapeDtypeStruct((ROWS, D), BF16),
+            jax.ShapeDtypeStruct((ROWS, D), BF16),
+            jax.ShapeDtypeStruct((16, D), F32),
+            jax.ShapeDtypeStruct((TAPS, 128), F32),
+            jax.ShapeDtypeStruct((1, 128), F32),
+        ),
+        in_specs=[hbm] * 4,
+        out_specs=(hbm,) * 5,
+        scratch_shapes=[
+            pltpu.VMEM((ROWS, D), BF16),
+            pltpu.VMEM((ROWS, D), BF16),
+            pltpu.VMEM((16, D), F32),
+            pltpu.VMEM((32, 128), F32),
+            pltpu.VMEM((TAPS, 128), F32),
+            pltpu.VMEM((1, 128), F32),
+            pltpu.SemaphoreType.DMA((10,)),
+            pltpu.SemaphoreType.DMA((11,)),
+        ],
+    )(grad_value, grad_gate, grad_weight, grad_taps)
+    return (grad_value[None], grad_gate[None], grad_weight, grad_kernel, grad_gain[0])
 
 
 def solution(mesh):

time: 78.3 us -> 65.9 us (0.84)
  local copies, waits for them, and re-layouts: 5.94 us -> 0 us
  Pallas kernels: 70.8 us -> 65.1 us
    pallas_call x1, Pallas kernels: 70.8 us -> 62.6 us  [shards(): pl.pallas_call(kernel, out_shape=(jax.ShapeDtypeStruct((ROWS, D), BF16),...]
    unnamed x10 -> x0, local copies, waits for them, and re-layouts: 4.74 us -> none
    pallas_call x0 -> x1, Pallas kernels: none -> 2.5 us  [shards(): pl.pallas_call(place, out_shape=(jax.ShapeDtypeStruct((ROWS, D), BF16), j...]
    squeeze x1 -> x0, local copies, waits for them, and re-layouts: 1.2 us -> none  [shards(): grad_taps[TAPS]]
where the time goes in v2:
time: 65.9 us; the launch traced here: 65.7 us
  Pallas kernels  65.1 us (99%)
    pallas_call x1, Pallas kernels, shards(): pl.pallas_call(kernel, out_shape=(jax.ShapeDtypeStruct((ROWS, D), BF16),...  62.6 us
    pallas_call x1, Pallas kernels, shards(): pl.pallas_call(place, out_shape=(jax.ShapeDtypeStruct((ROWS, D), BF16), j...  2.5 us

profile of v2, /device:TPU:1, one launch (start us, length us, event | category | flops | bytes accessed | tf_op | source)
XLA Modules:
  0.0 65.7 jit_solution(3465135697226976787)
XLA Ops:
  0.6 62.6 %shard_map.101 = (bf16[256,2048]{1,0:T(8,128)(2,1)}, bf16[256,2048]{1,0:T(8,128)(2,1)}, f32[16,2048]{1,0:T(8,128)}, f32[32,128]{1,0:T(8,128)}) custom-call(bf16[256,2048]{1,0:T(8,128)(2,1)} %bitcast.7, bf16[256,2048]{1,0:T(8,128)(2,1)} %bitcast.8, bf16[256,2048]{1,0:T(8,128)(2,1)} %bitcast.9, bf16[256,2048]{1,0:T(8,128)(2,1)} %w_hbm.1, ...), custom_call_target="tpu_custom_call" | custom-call | tf_op jit(solution)/shard_map/pallas_call | solution.py:782
  63.2 2.5 %shard_map.102 = (bf16[256,2048]{1,0:T(8,128)(2,1)}, bf16[256,2048]{1,0:T(8,128)(2,1)}, f32[16,2048]{1,0:T(8,128)}, f32[31,128]{1,0:T(8,128)}, f32[1,128]{1,0:T(1,128)}) custom-call(bf16[256,2048]{1,0:T(8,128)(2,1)} %get-tuple-element.14.gv_in, bf16[256,2048]{1,0:T(8,128)(2,1)} %get-tuple-element.15.gg_in, f32[16,2048]{1,0:T(8,128)} %get-tuple-element.16.ow_in, ...), custom_call_target="tpu_custom_call" | custom-call | tf_op jit(solution)/shard_map/pallas_call | solution.py:798

commit v3 on v2

--- a/solution.py
+++ b/solution.py
@@ -19,8 +19,8 @@
 TAPS = 31
 NSP = 16
 NDP = 8
-WX_COLS, WY_COLS, WZ_COLS = (0, 512), (512, 768), (1280, 768)
-COLOURS = ((0, 384), (384, 384), (768, 256))
+WX_COLS, WY_COLS, WZ_COLS = (0, 384), (384, 896), (1280, 768)
+COLOURS = ((0, 384), (384, 256), (640, 384))
 
 TAP0 = 0
 COT0 = TAP0 + 16
@@ -33,11 +33,10 @@
 RA0 = GA0 + 4
 RB0 = RA0 + 18
 RC0 = RB0 + 9
-GK0 = RC0 + 9
+GK0 = RC0 + 21
 GD0 = GK0 + 16
 GC0 = GD0 + 8
-FIN0 = GC0 + 1
-NSEM = FIN0 + 1
+NSEM = GC0 + 1
 
 
 def sigmoid(x):
@@ -65,8 +64,8 @@
     val_hbm,
     gate_hbm,
     w_hbm,
-    taps_in,
-    gain_in,
+    taps_hbm,
+    gain_hbm,
     gv_hbm,
     gg_hbm,
     ow_ref,
@@ -122,9 +121,9 @@
     r3b,
     r3c,
     finp,
-    fins,
-    finr,
     perm,
+    taps_in,
+    gain_in,
     ssem,
     rsem,
     lsem,
@@ -134,12 +133,16 @@
     z, y = s // 4, s % 4
     x, q = d // 2, d % 2
 
-    def at(axis, off):
+    def at(axis, off, core=None):
+        dp = d if core is None else x * 2 + core
         if axis == 0:
-            return {"sp": s, "dp": ((x + off) % 4) * 2 + q}
+            return {"sp": s, "dp": ((x + off) % 4) * 2 + (q if core is None else core)}
         if axis == 1:
-            return {"sp": z * 4 + (y + off) % 4, "dp": d}
-        return {"sp": ((z + off) % 4) * 4 + y, "dp": d}
+            return {"sp": z * 4 + (y + off) % 4, "dp": dp}
+        return {"sp": ((z + off) % 4) * 4 + y, "dp": dp}
+
+    def slot(axis, off):
+        return (off - 1) % 4 if axis == 2 else (coord[axis] + off) % 4
 
     partner = {"sp": s, "dp": x * 2 + (1 - q)}
     coord = (x, y, z)
@@ -165,7 +168,11 @@
         pltpu.make_async_copy(gate_hbm, gate, lsem.at[2]),
         pltpu.make_async_copy(cot_hbm, cotraw.at[q], lsem.at[3]),
     ]
-    for c in local:
+    small = [
+        pltpu.make_async_copy(taps_hbm, taps_in, lsem.at[12]),
+        pltpu.make_async_copy(gain_hbm, gain_in, lsem.at[13]),
+    ]
+    for c in (local[0], *small, *local[1:]):
         c.start()
     barrier = pltpu.get_barrier_semaphore()
 
@@ -177,13 +184,13 @@
 
     loop(NSP - 1, greet_sp)
     loop(NDP - 1, greet_dp)
-    tkown[0:TAPS, :] = taps_in[...].astype(F32)
-    tkown[TAPS : TAPS + 1, :] = gain_in[...].astype(F32)
-    tkall[s] = tkown[...].astype(BF16)
+    for axis in (1, 2):
+        for r in (1, 2, 3):
+            pl.semaphore_signal(barrier, inc=1, device_id=at(axis, r, 1 - q), device_id_type=MESH)
     r_io = lax.broadcasted_iota(jnp.int32, (ROWS, ROWS), 0)
     t_io = lax.broadcasted_iota(jnp.int32, (ROWS, ROWS), 1)
     perm[...] = jnp.where(t_io == (r_io & 15) * SEG + (r_io >> 4), 1.0, 0.0).astype(BF16)
-    pl.semaphore_wait(barrier, NSP - 1 + NDP - 1)
+    pl.semaphore_wait(barrier, NSP - 1 + NDP - 1 + 6)
 
     def piece(cols, size):
         def at_quarter(xx, quarter, h=None):
@@ -199,6 +206,12 @@
         send(wy(x, y), wy(x, y), WX0 + i, at(0, off))
     for i, off in ((0, 1), (1, -1)):
         send(wz(x, z), wz(x, z), WX0 + 2 + i, at(0, off))
+
+    for c in small:
+        c.wait()
+    tkown[0:TAPS, :] = taps_in[...].astype(F32)
+    tkown[TAPS : TAPS + 1, :] = gain_in[...].astype(F32)
+    tkall[s] = tkown[...].astype(BF16)
 
     def send_taps(r):
         copy(tkall.at[s], tkall.at[s], TAP0 + r, {"sp": (s + r + 1) % NSP, "dp": d}).start()
@@ -257,37 +270,6 @@
         for i, _ in both:
             got(part(xx, (here + 2) % 4, i), base + 4 * pos + 2 + i)
 
-    def weights1():
-        along_x(wy, y, 0)
-        across(1, left, 0)
-        across(1, right, 1)
-
-    def weights2():
-        along_x(wz, z, 2)
-        across(2, left, 0)
-        across(2, right, 1)
-        for i, off in both:
-            send(wx(x, 0), wx(x, 0), WX0 + 4 + i, at(0, off))
-
-    def weights3():
-        far_along_x(wy, y, 0)
-        across(1, far, 2)
-        across_on(1, left, 0)
-
-    def weights4():
-        far_along_x(wz, z, 2)
-        across(2, far, 2)
-        across_on(1, right, 1)
-        across_on(2, left, 0)
-
-    def weights5():
-        across_on(2, right, 1)
-        across_on(1, far, 2)
-        along_x(wx, 0, 4)
-
-    def weights6():
-        across_on(2, far, 2)
-
     def weights_end(xx, pos):
         across_end(1, xx, pos)
         across_end(2, xx, pos)
@@ -324,7 +306,9 @@
     def _():
         gext[0:32, :] = jnp.zeros((32, D), BF16)
 
-    weights1()
+    along_x(wy, y, 0)
+    across(1, left, 0)
+    across(1, right, 1)
     spread(gext, 16, ext, ROWS)
     spread(gext, 0, ext, 0)
 
@@ -362,9 +346,15 @@
 
         filtered(col, ext, lambda j, k: j - k + 2 * SEG, emit)
 
+    along_x(wz, z, 2)
+    across(2, left, 0)
+    across(2, right, 1)
+    for i, off in both:
+        send(wx(x, 0), wx(x, 0), WX0 + 4 + i, at(0, off))
     loop(NSP, conv_block)
 
-    weights2()
+    far_along_x(wy, y, 0)
+    across(1, far, 2)
 
     def conv_sums(j):
         at_rows = rows(j, 16)
@@ -385,8 +375,9 @@
     def act_block(g, j):
         at_rows = rows(j, 16)
         m, iv = sum1[at_rows, :], inv_b[at_rows, :]
-        for col in range(4 * g, 4 * g + 4):
-            ln = pl.ds(128 * col, 128)
+        for i in range(4):
+            col = 4 * g + i
+            ln = lanes(col)
             centred = (cen[col, at_rows, :] - m) * iv
             cen[col, at_rows, :] = centred
             normed = centred * gains[:, ln]
@@ -394,48 +385,85 @@
             act[pl.ds(pl.multiple_of(q * ROWS + j * 16, 16), 16), ln] = (normed * sg).astype(BF16)
             fwd[col, at_rows, :] = sg * (1.0 + normed * (1.0 - sg))
 
-    for g in range(4):
-        loop(SEG, lambda j: act_block(g, j))
-        part = act.at[rows(q, ROWS), pl.ds(512 * g, 512)]
-        send(part, part, ACT0 + g, partner)
-        if g == 1:
-            weights3()
-
-    weights4()
+    order = (1, 0, 2, 3)
+    groups = [(z + 1 + zr) % 4 for zr in order]
+    for pos, g in enumerate(groups):
+        loop(SEG, lambda j, g=g: act_block(g, j))
+        part = act.at[rows(q, ROWS), lanes(g, 512)]
+        send(part, part, ACT0 + pos, partner)
+        if pos == 1:
+            across_on(1, left, 0)
+        if pos == 3:
+            far_along_x(wz, z, 2)
+            across(2, far, 2)
 
     blocks = (pa, pb, pc)
     half = lanes(q, HALF)
 
-    def outer(cb):
+    def outer(g, zr, i):
         p = lax.dot_general(
-            act[:, lanes(cb, 256)], cotp[:, half], (((0,), (0,)), ((), ())), preferred_element_type=F32
+            act[:, lanes(2 * g + i, 256)], cotp[:, half], (((0,), (0,)), ((), ())), preferred_element_type=F32
         ).astype(BF16)
-        zz, y0 = cb // 2, (cb % 2) * 2
-        for i in range(8):
-            yy, xx = y0 + i // 4, i % 4
-            piece = p[32 * i : 32 * i + 32]
-            pa[xx, yy, zz] = piece[:, 0:384]
-            pb[yy, zz, xx] = piece[:, 384:768]
-            pc[zz, xx, yy] = piece[:, 768:1024]
-
-    for g in range(4):
-        got(act.at[rows(1 - q, ROWS), pl.ds(512 * g, 512)], ACT0 + g)
-        loop(2, lambda i: outer(i + 2 * g))
-        if g == 1:
-            weights5()
+        for n in range(8):
+            yy, xx = i * 2 + n // 4, n % 4
+            part = p[32 * n : 32 * n + 32]
+            pa[xx, yy, zr] = part[:, 0:384]
+            pb[yy, zr, xx] = part[:, 384:640]
+            pc[zr, xx, yy] = part[:, 640:1024]
 
     r1s, cbs = (r1a, r1b, r1c), (cba, cbb, cbc)
     s1s, r2s, s2s, r3s = (s1a, s1b, s1c), (r2a, r2b, r2c), (s2a, s2b, s2c), (r3a, r3b, r3c)
-    lo, hi = pl.ds(0, 2), pl.ds(2, 2)
-    weights6()
-    for c in range(3):
-        me = coord[c]
-        send(blocks[c].at[(me + 2) % 4, lo], r1s[c].at[0], RA0 + 6 * c, at(c, 1))
-        send(blocks[c].at[(me + 2) % 4, hi], r1s[c].at[1], RA0 + 6 * c + 1, at(c, -1))
-    for c in range(3):
-        me = coord[c]
-        send(blocks[c].at[(me + 1) % 4, hi], r1s[c].at[2], RA0 + 6 * c + 2, at(c, 1))
-        send(blocks[c].at[(me + 3) % 4, lo], r1s[c].at[3], RA0 + 6 * c + 3, at(c, -1))
+    firsts, lasts = pl.ds(0, 2), pl.ds(2, 2)
+
+    def half_of(c, off, h):
+        cut = (firsts, lasts)[h]
+        if c == 0:
+            return blocks[0].at[slot(0, off), :, cut]
+        return blocks[c].at[slot(c, off), cut]
+
+    def sums_far(c, h):
+        send(half_of(c, 2, h), r1s[c].at[h], RA0 + 6 * c + h, at(c, (1, -1)[h]))
+
+    def sums_alone(c, h):
+        send(half_of(c, (-1, 1)[h], h), r1s[c].at[3 - h], RA0 + 6 * c + 3 - h, at(c, (-1, 1)[h]))
+
+    for pos, (g, zr) in enumerate(zip(groups, order)):
+        got(act.at[rows(1 - q, ROWS), lanes(g, 512)], ACT0 + pos)
+        loop(2, lambda i, g=g, zr=zr: outer(g, zr, i))
+        if pos == 0:
+            across_on(2, left, 0)
+            sums_far(2, 0)
+            sums_far(2, 1)
+        if pos == 1:
+            across_on(1, right, 1)
+            for c in (0, 1):
+                sums_far(c, 0)
+                sums_alone(c, 0)
+        if pos == 2:
+            across_on(2, right, 1)
+        if pos == 3:
+            across_on(1, far, 2)
+            across_on(2, far, 2)
+            along_x(wx, 0, 4)
+            for c in (0, 1):
+                sums_far(c, 1)
+            for c in (0, 1):
+                sums_alone(c, 1)
+            sums_alone(2, 0)
+            sums_alone(2, 1)
+
+    def each(c, body):
+        loop(8, (lambda i: body(i // 2, i % 2)) if c == 0 else (lambda i: body(i // 4, i % 4)))
+
+    def join(c, h):
+        got(r1s[c].at[h], RA0 + 6 * c + h)
+        own = half_of(c, (1, -1)[h], h)
+
+        def add(a, b):
+            cbs[c][h, a, b] = (own[a, b].astype(F32) + r1s[c][h, a, b].astype(F32)).astype(BF16)
+
+        each(c, add)
+        send(cbs[c].at[h], r1s[c].at[4 + h], RA0 + 6 * c + 4 + h, at(c, (1, -1)[h]))
 
     def back_send(pos, xx):
         blk = xx * 2 + q
@@ -449,25 +477,14 @@
     back_send(0, left)
     weights_end(right, 1)
     back_send(1, right)
+    join(2, 0)
+    join(2, 1)
     weights_end(far, 2)
     back_send(2, far)
 
-    def join(c):
-        me = coord[c]
-        for h, idx, off in ((lo, 0, 1), (hi, 1, -1)):
-            got(r1s[c].at[idx], RA0 + 6 * c + idx)
-            own = blocks[c].at[(me + off) % 4, h]
-
-            def add(i, own=own, idx=idx):
-                a, b = i // 4, i % 4
-                total = own[a, b].astype(F32) + r1s[c][idx, a, b].astype(F32)
-                cbs[c][idx, a, b] = total.astype(BF16)
-
-            loop(8, add)
-            send(cbs[c].at[idx], r1s[c].at[4 + idx], RA0 + 6 * c + 4 + idx, at(c, off))
-
-    for c in range(3):
-        join(c)
+    for c in (1, 0):
+        join(c, 0)
+        join(c, 1)
 
     for pos, off in ((3, 0), (0, 3), (1, 1), (2, 2)):
         got(ga.at[((x + off) % 4) * 2 + 1 - q], GA0 + pos)
@@ -546,25 +563,21 @@
     loop(NSP - 1, send_gk)
 
     def stage1(c):
-        got(r1s[c].at[2], RA0 + 6 * c + 2)
-        got(r1s[c].at[3], RA0 + 6 * c + 3)
-        got(r1s[c].at[4], RA0 + 6 * c + 4)
-        got(r1s[c].at[5], RA0 + 6 * c + 5)
-        me = coord[c]
-
-        def add(i):
-            a, b = i // 4, i % 4
-            s1s[c][a, b] = (
-                blocks[c][me, a, b].astype(F32) + r1s[c][4, a, b].astype(F32) + r1s[c][3, a, b].astype(F32)
-            ).astype(BF16)
-            s1s[c][a + 2, b] = (
-                blocks[c][me, a + 2, b].astype(F32) + r1s[c][2, a, b].astype(F32) + r1s[c][5, a, b].astype(F32)
-            ).astype(BF16)
-
-        loop(8, add)
+        for n in range(2, 6):
+            got(r1s[c].at[n], RA0 + 6 * c + n)
+        for h, pair in ((0, (4, 3)), (1, (2, 5))):
+            own = half_of(c, 0, h)
+            dst = s1s[c].at[:, (firsts, lasts)[h]] if c == 0 else s1s[c].at[(firsts, lasts)[h]]
+
+            def add(a, b, own=own, dst=dst, pair=pair):
+                dst[a, b] = (
+                    own[a, b].astype(F32) + r1s[c][pair[0], a, b].astype(F32) + r1s[c][pair[1], a, b].astype(F32)
+                ).astype(BF16)
+
+            each(c, add)
         axis = (c + 1) % 3
         for r in range(1, 4):
-            send(s1s[c].at[(coord[axis] + r) % 4], r2s[c].at[r - 1], RB0 + 3 * c + r - 1, at(axis, r))
+            send(s1s[c].at[slot(axis, r)], r2s[c].at[r - 1], RB0 + 3 * c + r - 1, at(axis, r))
 
     def stage2(c):
         axis, last = (c + 1) % 3, (c + 2) % 3
@@ -572,36 +585,43 @@
             got(r2s[c].at[r - 1], RB0 + 3 * c + r - 1)
 
         def add(i):
-            total = s1s[c][coord[axis], i].astype(F32)
+            total = s1s[c][slot(axis, 0), i].astype(F32)
             for r in range(3):
                 total = total + r2s[c][r, i].astype(F32)
             s2s[c][i] = total.astype(BF16)
 
         loop(4, add)
         for r in range(1, 4):
-            send(s2s[c].at[(coord[last] + r) % 4], r3s[c].at[r - 1], RC0 + 3 * c + r - 1, at(last, r))
+            for other in range(2):
+                core = 1 - q if other else q
+                send(
+                    s2s[c].at[slot(last, r), rows(core, 16)],
+                    r3s[c].at[other, r],
+                    RC0 + 7 * c + 2 * r + other - 1,
+                    at(last, r, core),
+                )
+        send(s2s[c].at[slot(last, 0), rows(1 - q, 16)], r3s[c].at[1, 0], RC0 + 7 * c, partner)
 
     factor = float(NSP * NDP * ROWS) ** (-0.5)
 
     def stage3(c):
         last = (c + 2) % 3
         first, size = COLOURS[c]
+        got(r3s[c].at[1, 0], RC0 + 7 * c)
         for r in range(1, 4):
-            got(r3s[c].at[r - 1], RC0 + 3 * c + r - 1)
-        mine = coord[last]
-        for to_partner in (False, True):
-            h = (1 - q) if to_partner else q
-            part = rows(h, 16)
-            total = s2s[c][mine, part, :].astype(F32)
-            for r in range(3):
-                total = total + r3s[c][r, part, :].astype(F32)
-            total = total * factor
-            if to_partner:
-                fins[:, first : first + size] = total
+            for other in range(2):
+                got(r3s[c].at[other, r], RC0 + 7 * c + 2 * r + other - 1)
+        for other in range(2):
+            if other:
+                total = r3s[c][1, 0].astype(F32)
             else:
-                ow_ref[:, pl.ds(pl.multiple_of(q * HALF + first, 128), size)] = total
-
-    for c in range(3):
+                total = s2s[c][slot(last, 0), rows(q, 16), :].astype(F32)
+            for r in range(1, 4):
+                total = total + r3s[c][other, r].astype(F32)
+            core = 1 - q if other else q
+            ow_ref[:, pl.ds(pl.multiple_of(core * HALF + first, 128), size)] = total * factor
+
+    for c in (2, 1, 0):
         stage1(c)
 
     @pl.when(s < NSP - 1)
@@ -658,13 +678,12 @@
 
     loop(NDP - 1, send_gd)
     group(1)
-    for c in range(3):
+    for c in (2, 1, 0):
         stage2(c)
     group(2)
-    for c in range(3):
+    group(3)
+    for c in (2, 1, 0):
         stage3(c)
-    send(fins, finr, FIN0, partner)
-    group(3)
 
     def got_gd(r):
         got(gdr.at[r], GD0 + r)
@@ -674,8 +693,6 @@
     for r in range(NDP - 1):
         total = total + gdr[r]
     gk_ref[...] = total * factor
-    got(finr, FIN0)
-    ow_ref[:, lanes(1 - q, HALF)] = finr[...]
 
     for c in sent:
         c.wait_send()
@@ -767,17 +784,18 @@
         ((NDP - 1, 32, 128), F32),
     ]
     scratch += [((4, 4, 4, 32, f), BF16) for f in sizes]
-    scratch += [((6, 2, 4, 32, f), BF16) for f in sizes]
-    scratch += [((2, 2, 4, 32, f), BF16) for f in sizes]
+    halves = [(4, 2), (2, 4), (2, 4)]
+    scratch += [((6, *h, 32, f), BF16) for h, f in zip(halves, sizes)]
+    scratch += [((2, *h, 32, f), BF16) for h, f in zip(halves, sizes)]
     scratch += [((4, 4, 32, f), BF16) for f in sizes]
     scratch += [((3, 4, 32, f), BF16) for f in sizes]
     scratch += [((4, 32, f), BF16) for f in sizes]
-    scratch += [((3, 32, f), BF16) for f in sizes]
+    scratch += [((2, 4, 16, f), BF16) for f in sizes]
     scratch += [
         ((4, 2 * ROWS, ROWS), BF16),
-        ((16, HALF), F32),
-        ((16, HALF), F32),
         ((ROWS, ROWS), BF16),
+        ((TAPS, 128), BF16),
+        ((1, 128), BF16),
     ]
     grad_value, grad_gate, grad_weight, grad_taps = pl.pallas_call(
         kernel,
@@ -787,10 +805,10 @@
             jax.ShapeDtypeStruct((16, D), F32),
             jax.ShapeDtypeStruct((32, 128), F32),
         ),
-        in_specs=[hbm, hbm, hbm, hbm, vmem, vmem],
+        in_specs=[pl.BlockSpec(memory_space=pltpu.HBM)] * 6,
         out_specs=(hbm, hbm, vmem, vmem),
         scratch_shapes=[pltpu.VMEM(shape, kind) for shape, kind in scratch]
-        + [pltpu.SemaphoreType.DMA((NSEM,)), pltpu.SemaphoreType.DMA((NSEM,)), pltpu.SemaphoreType.DMA((12,))],
+        + [pltpu.SemaphoreType.DMA((NSEM,)), pltpu.SemaphoreType.DMA((NSEM,)), pltpu.SemaphoreType.DMA((14,))],
         compiler_params=pltpu.CompilerParams(
             collective_id=0, has_side_effects=True, vmem_limit_bytes=60 * 1024 * 1024
         ),

time: 65.9 us -> 60.9 us (0.924)
  Pallas kernels: 65.1 us -> 60.1 us
    pallas_call x1, Pallas kernels: 62.6 us -> 57.6 us  [shards(): pl.pallas_call(kernel, out_shape=(jax.ShapeDtypeStruct((ROWS, D), BF16),...]
where the time goes in v3:
time: 60.9 us; the launch traced here: 60.7 us
  Pallas kernels  60.1 us (99%)
  between operations  0.64 us (1%)
    pallas_call x1, Pallas kernels, shards(): pl.pallas_call(kernel, out_shape=(jax.ShapeDtypeStruct((ROWS, D), BF16),...  57.6 us
    pallas_call x1, Pallas kernels, shards(): pl.pallas_call(place, out_shape=(jax.ShapeDtypeStruct((ROWS, D), BF16), j...  2.5 us

profile of v3, /device:TPU:1, one launch (start us, length us, event | category | flops | bytes accessed | tf_op | source)
XLA Modules:
  0.0 60.7 jit_solution(11037924379208756136)
XLA Ops:
  0.6 57.6 %shard_map.101 = (bf16[256,2048]{1,0:T(8,128)(2,1)}, bf16[256,2048]{1,0:T(8,128)(2,1)}, f32[16,2048]{1,0:T(8,128)}, f32[32,128]{1,0:T(8,128)}) custom-call(bf16[256,2048]{1,0:T(8,128)(2,1)} %bitcast.7, bf16[256,2048]{1,0:T(8,128)(2,1)} %bitcast.8, bf16[256,2048]{1,0:T(8,128)(2,1)} %bitcast.9, bf16[256,2048]{1,0:T(8,128)(2,1)} %w_hbm.1, ...), custom_call_target="tpu_custom_call" | custom-call | tf_op jit(solution)/shard_map/pallas_call | solution.py:800
  58.2 2.5 %shard_map.102 = (bf16[256,2048]{1,0:T(8,128)(2,1)}, bf16[256,2048]{1,0:T(8,128)(2,1)}, f32[16,2048]{1,0:T(8,128)}, f32[31,128]{1,0:T(8,128)}, f32[1,128]{1,0:T(1,128)}) custom-call(bf16[256,2048]{1,0:T(8,128)(2,1)} %get-tuple-element.14.gv_in, bf16[256,2048]{1,0:T(8,128)(2,1)} %get-tuple-element.15.gg_in, f32[16,2048]{1,0:T(8,128)} %get-tuple-element.16.ow_in, ...), custom_call_target="tpu_custom_call" | custom-call | tf_op jit(solution)/shard_map/pallas_call | solution.py:816

commit v4 on v3

--- a/solution.py
+++ b/solution.py
@@ -25,14 +25,14 @@
 TAP0 = 0
 COT0 = TAP0 + 16
 HALO0 = COT0 + 1
-WX0 = HALO0 + 1
+WX0 = HALO0 + 2
 WY0 = WX0 + 12
 WZ0 = WY0 + 12
 ACT0 = WZ0 + 12
 GA0 = ACT0 + 4
 RA0 = GA0 + 4
 RB0 = RA0 + 18
-RC0 = RB0 + 9
+RC0 = RB0 + 18
 GK0 = RC0 + 21
 GD0 = GK0 + 16
 GC0 = GD0 + 8
@@ -229,12 +229,19 @@
 
     gate_block(0)
 
-    def halo_copy():
-        return copy(gext.at[pl.ds(ROWS, 32)], gext.at[pl.ds(0, 32)], HALO0, {"sp": (s + 1) % NSP, "dp": d})
+    def halo_copy(n):
+        cols = pl.ds(HALF * n, HALF)
+        return copy(
+            gext.at[pl.ds(ROWS, 32), cols],
+            gext.at[pl.ds(0, 32), cols],
+            HALO0 + n,
+            {"sp": (s + 1) % NSP, "dp": d},
+        )
 
     @pl.when(s < NSP - 1)
     def _():
-        halo_copy().start()
+        halo_copy(0).start()
+        halo_copy(1).start()
 
     local[3].wait()
     send(cotraw.at[q], cotraw.at[q], COT0, partner)
@@ -276,14 +283,14 @@
         if pos == 2:
             far_along_x(wx, 0, 4)
 
+    def spread_half(src, first, dst, base, n):
+        block = jnp.dot(perm[...], src[pl.ds(first, ROWS), lanes(n, HALF)], preferred_element_type=F32)
+        block = block.astype(BF16)
+        for i in range(8):
+            dst[n * 8 + i, pl.ds(base, ROWS), :] = block[:, 128 * i : 128 * i + 128]
+
     def spread(src, first, dst, base):
-        def body(n):
-            block = jnp.dot(perm[...], src[pl.ds(first, ROWS), lanes(n, 1024)], preferred_element_type=F32)
-            block = block.astype(BF16)
-            for i in range(8):
-                dst[n * 8 + i, pl.ds(base, ROWS), :] = block[:, 128 * i : 128 * i + 128]
-
-        loop(2, body)
+        loop(2, lambda n: spread_half(src, first, dst, base, n))
 
     spread(gext, 32, ext, 2 * ROWS)
 
@@ -298,33 +305,30 @@
     got(cotraw.at[1 - q], COT0)
     spread_cot(1 - q)
 
-    @pl.when(s > 0)
-    def _():
-        got(gext.at[pl.ds(0, 32)], HALO0)
-
-    @pl.when(s == 0)
-    def _():
-        gext[0:32, :] = jnp.zeros((32, D), BF16)
-
-    along_x(wy, y, 0)
-    across(1, left, 0)
-    across(1, right, 1)
-    spread(gext, 16, ext, ROWS)
-    spread(gext, 0, ext, 0)
+    def halo_in(n):
+        cols = pl.ds(HALF * n, HALF)
+
+        @pl.when(s > 0)
+        def _():
+            got(gext.at[pl.ds(0, 32), cols], HALO0 + n)
+
+        @pl.when(s == 0)
+        def _():
+            gext[0:32, cols] = jnp.zeros((32, HALF), BF16)
+
+    def spread_before(n):
+        spread_half(gext, 16, ext, ROWS, n)
+        spread_half(gext, 0, ext, 0, n)
 
     def got_taps(r):
         src = (s + NSP - 1 - r) % NSP
         got(tkall.at[src], TAP0 + r)
-
-    loop(NSP - 1, got_taps)
 
     def widen(i):
         t = tkall[i].astype(F32)
         gains[:, lanes(i)] = jnp.broadcast_to(t[TAPS : TAPS + 1], (16, 128))
         for k in range(TAPS):
             taps[i, 16 * k : 16 * k + 16, :] = jnp.broadcast_to(t[k : k + 1], (16, 128)).astype(BF16)
-
-    loop(NSP, widen)
 
     def filtered(col, src, shift, emit):
         tiles, weights = src.at[col], taps.at[col]
@@ -346,15 +350,23 @@
 
         filtered(col, ext, lambda j, k: j - k + 2 * SEG, emit)
 
+    halo_in(0)
+    spread_before(0)
+    along_x(wy, y, 0)
+    across(1, left, 0)
+    across(1, right, 1)
+    loop(NSP - 1, got_taps)
+    loop(NSP, widen)
+    loop(8, conv_block)
     along_x(wz, z, 2)
     across(2, left, 0)
     across(2, right, 1)
     for i, off in both:
         send(wx(x, 0), wx(x, 0), WX0 + 4 + i, at(0, off))
-    loop(NSP, conv_block)
-
-    far_along_x(wy, y, 0)
-    across(1, far, 2)
+    halo_in(1)
+    spread_before(1)
+    loop(8, lambda i: conv_block(i + 8))
+
 
     def conv_sums(j):
         at_rows = rows(j, 16)
@@ -391,9 +403,11 @@
         loop(SEG, lambda j, g=g: act_block(g, j))
         part = act.at[rows(q, ROWS), lanes(g, 512)]
         send(part, part, ACT0 + pos, partner)
-        if pos == 1:
+        if pos == 2:
+            far_along_x(wy, y, 0)
+            across(1, far, 2)
+        if pos == 3:
             across_on(1, left, 0)
-        if pos == 3:
             far_along_x(wz, z, 2)
             across(2, far, 2)
 
@@ -417,9 +431,9 @@
 
     def half_of(c, off, h):
         cut = (firsts, lasts)[h]
-        if c == 0:
-            return blocks[0].at[slot(0, off), :, cut]
-        return blocks[c].at[slot(c, off), cut]
+        if c == 1:
+            return blocks[c].at[slot(c, off), cut]
+        return blocks[c].at[slot(c, off), :, cut]
 
     def sums_far(c, h):
         send(half_of(c, 2, h), r1s[c].at[h], RA0 + 6 * c + h, at(c, (1, -1)[h]))
@@ -430,30 +444,29 @@
     for pos, (g, zr) in enumerate(zip(groups, order)):
         got(act.at[rows(1 - q, ROWS), lanes(g, 512)], ACT0 + pos)
         loop(2, lambda i, g=g, zr=zr: outer(g, zr, i))
-        if pos == 0:
+        if pos == 1:
             across_on(2, left, 0)
-            sums_far(2, 0)
-            sums_far(2, 1)
-        if pos == 1:
             across_on(1, right, 1)
-            for c in (0, 1):
-                sums_far(c, 0)
-                sums_alone(c, 0)
+            sums_far(0, 0)
+            sums_alone(0, 0)
         if pos == 2:
             across_on(2, right, 1)
         if pos == 3:
+            along_x(wx, 0, 4)
+            sums_far(0, 1)
             across_on(1, far, 2)
+            sums_far(1, 0)
+            sums_far(1, 1)
             across_on(2, far, 2)
-            along_x(wx, 0, 4)
-            for c in (0, 1):
-                sums_far(c, 1)
-            for c in (0, 1):
+            sums_far(2, 0)
+            sums_far(2, 1)
+            for c in (2, 1):
+                sums_alone(c, 0)
                 sums_alone(c, 1)
-            sums_alone(2, 0)
-            sums_alone(2, 1)
+            sums_alone(0, 1)
 
     def each(c, body):
-        loop(8, (lambda i: body(i // 2, i % 2)) if c == 0 else (lambda i: body(i // 4, i % 4)))
+        loop(8, (lambda i: body(i // 4, i % 4)) if c == 1 else (lambda i: body(i // 2, i % 2)))
 
     def join(c, h):
         got(r1s[c].at[h], RA0 + 6 * c + h)
@@ -477,14 +490,15 @@
     back_send(0, left)
     weights_end(right, 1)
     back_send(1, right)
+    join(0, 0)
+    weights_end(far, 2)
+    back_send(2, far)
+
+    join(1, 0)
+    join(1, 1)
     join(2, 0)
     join(2, 1)
-    weights_end(far, 2)
-    back_send(2, far)
-
-    for c in (1, 0):
-        join(c, 0)
-        join(c, 1)
+    join(0, 1)
 
     for pos, off in ((3, 0), (0, 3), (1, 1), (2, 2)):
         got(ga.at[((x + off) % 4) * 2 + 1 - q], GA0 + pos)
@@ -562,27 +576,35 @@
 
     loop(NSP - 1, send_gk)
 
-    def stage1(c):
-        for n in range(2, 6):
+    def stage1(c, h):
+        pair = ((4, 3), (2, 5))[h]
+        for n in pair:
             got(r1s[c].at[n], RA0 + 6 * c + n)
-        for h, pair in ((0, (4, 3)), (1, (2, 5))):
-            own = half_of(c, 0, h)
-            dst = s1s[c].at[:, (firsts, lasts)[h]] if c == 0 else s1s[c].at[(firsts, lasts)[h]]
-
-            def add(a, b, own=own, dst=dst, pair=pair):
-                dst[a, b] = (
-                    own[a, b].astype(F32) + r1s[c][pair[0], a, b].astype(F32) + r1s[c][pair[1], a, b].astype(F32)
-                ).astype(BF16)
-
-            each(c, add)
+        own, cut = half_of(c, 0, h), (firsts, lasts)[h]
+        dst = s1s[c].at[cut] if c == 1 else s1s[c].at[:, cut]
+
+        def add(a, b):
+            dst[a, b] = (
+                own[a, b].astype(F32) + r1s[c][pair[0], a, b].astype(F32) + r1s[c][pair[1], a, b].astype(F32)
+            ).astype(BF16)
+
+        each(c, add)
         axis = (c + 1) % 3
-        for r in range(1, 4):
-            send(s1s[c].at[slot(axis, r)], r2s[c].at[r - 1], RB0 + 3 * c + r - 1, at(axis, r))
+        for r in (2, 1, 3):
+            i = slot(axis, r)
+            if c != 1:
+                send(s1s[c].at[i, cut], r2s[c].at[r - 1, cut], RB0 + 6 * c + 2 * (r - 1) + h, at(axis, r))
+            elif i // 2 == h:
+                send(s1s[c].at[i], r2s[c].at[r - 1], RB0 + 6 * c + 2 * (r - 1), at(axis, r))
 
     def stage2(c):
         axis, last = (c + 1) % 3, (c + 2) % 3
         for r in range(1, 4):
-            got(r2s[c].at[r - 1], RB0 + 3 * c + r - 1)
+            if c == 1:
+                got(r2s[c].at[r - 1], RB0 + 6 * c + 2 * (r - 1))
+            else:
+                for h, cut in enumerate((firsts, lasts)):
+                    got(r2s[c].at[r - 1, cut], RB0 + 6 * c + 2 * (r - 1) + h)
 
         def add(i):
             total = s1s[c][slot(axis, 0), i].astype(F32)
@@ -591,7 +613,7 @@
             s2s[c][i] = total.astype(BF16)
 
         loop(4, add)
-        for r in range(1, 4):
+        for r in (2, 1, 3):
             for other in range(2):
                 core = 1 - q if other else q
                 send(
@@ -621,8 +643,9 @@
             core = 1 - q if other else q
             ow_ref[:, pl.ds(pl.multiple_of(core * HALF + first, 128), size)] = total * factor
 
-    for c in (2, 1, 0):
-        stage1(c)
+    for c in (1, 0, 2):
+        for h in range(2):
+            stage1(c, h)
 
     @pl.when(s < NSP - 1)
     def _():
@@ -664,6 +687,7 @@
 
     group(0)
 
+    group(1)
     def got_gk(r):
         got(gkr.at[r], GK0 + r)
 
@@ -677,12 +701,11 @@
         copy(gdo, gdr.at[r], GD0 + r, {"sp": s, "dp": (d + r + 1) % NDP}).start()
 
     loop(NDP - 1, send_gd)
-    group(1)
-    for c in (2, 1, 0):
-        stage2(c)
     group(2)
     group(3)
-    for c in (2, 1, 0):
+    for c in (1, 0, 2):
+        stage2(c)
+    for c in (1, 0, 2):
         stage3(c)
 
     def got_gd(r):
@@ -710,7 +733,8 @@
 
     @pl.when(s < NSP - 1)
     def _():
-        halo_copy().wait_send()
+        halo_copy(0).wait_send()
+        halo_copy(1).wait_send()
 
     @pl.when(s > 0)
     def _():
@@ -784,7 +808,7 @@
         ((NDP - 1, 32, 128), F32),
     ]
     scratch += [((4, 4, 4, 32, f), BF16) for f in sizes]
-    halves = [(4, 2), (2, 4), (2, 4)]
+    halves = [(4, 2), (2, 4), (4, 2)]
     scratch += [((6, *h, 32, f), BF16) for h, f in zip(halves, sizes)]
     scratch += [((2, *h, 32, f), BF16) for h, f in zip(halves, sizes)]
     scratch += [((4, 4, 32, f), BF16) for f in sizes]

time: 60.9 us -> 58.8 us (0.966)
  Pallas kernels: 60.1 us -> 58 us
    pallas_call x1, Pallas kernels: 57.6 us -> 55.5 us  [shards(): pl.pallas_call(kernel, out_shape=(jax.ShapeDtypeStruct((ROWS, D), BF16),...]
where the time goes in v4:
time: 58.8 us; the launch traced here: 58.7 us
  Pallas kernels  58 us (99%)
  between operations  0.64 us (1%)
    pallas_call x1, Pallas kernels, shards(): pl.pallas_call(kernel, out_shape=(jax.ShapeDtypeStruct((ROWS, D), BF16),...  55.5 us
    pallas_call x1, Pallas kernels, shards(): pl.pallas_call(place, out_shape=(jax.ShapeDtypeStruct((ROWS, D), BF16), j...  2.5 us

profile of v4, /device:TPU:1, one launch (start us, length us, event | category | flops | bytes accessed | tf_op | source)
XLA Modules:
  0.0 58.7 jit_solution(14645709884013002882)
XLA Ops:
  0.6 55.5 %shard_map.101 = (bf16[256,2048]{1,0:T(8,128)(2,1)}, bf16[256,2048]{1,0:T(8,128)(2,1)}, f32[16,2048]{1,0:T(8,128)}, f32[32,128]{1,0:T(8,128)}) custom-call(bf16[256,2048]{1,0:T(8,128)(2,1)} %bitcast.7, bf16[256,2048]{1,0:T(8,128)(2,1)} %bitcast.8, bf16[256,2048]{1,0:T(8,128)(2,1)} %bitcast.9, bf16[256,2048]{1,0:T(8,128)(2,1)} %w_hbm.1, ...), custom_call_target="tpu_custom_call" | custom-call | tf_op jit(solution)/shard_map/pallas_call | solution.py:824
  56.2 2.5 %shard_map.102 = (bf16[256,2048]{1,0:T(8,128)(2,1)}, bf16[256,2048]{1,0:T(8,128)(2,1)}, f32[16,2048]{1,0:T(8,128)}, f32[31,128]{1,0:T(8,128)}, f32[1,128]{1,0:T(1,128)}) custom-call(bf16[256,2048]{1,0:T(8,128)(2,1)} %get-tuple-element.14.gv_in, bf16[256,2048]{1,0:T(8,128)(2,1)} %get-tuple-element.15.gg_in, f32[16,2048]{1,0:T(8,128)} %get-tuple-element.16.ow_in, ...), custom_call_target="tpu_custom_call" | custom-call | tf_op jit(solution)/shard_map/pallas_call | solution.py:840

commit v5 on v4

--- a/solution.py
+++ b/solution.py
@@ -190,34 +190,6 @@
     r_io = lax.broadcasted_iota(jnp.int32, (ROWS, ROWS), 0)
     t_io = lax.broadcasted_iota(jnp.int32, (ROWS, ROWS), 1)
     perm[...] = jnp.where(t_io == (r_io & 15) * SEG + (r_io >> 4), 1.0, 0.0).astype(BF16)
-    pl.semaphore_wait(barrier, NSP - 1 + NDP - 1 + 6)
-
-    def piece(cols, size):
-        def at_quarter(xx, quarter, h=None):
-            n, first = (size, quarter * size) if h is None else (size // 2, quarter * size + h * (size // 2))
-            return wg.at[xx, pl.ds(pl.multiple_of(first, n), n), pl.ds(*cols)]
-
-        return at_quarter
-
-    wx, wy, wz = piece(WX_COLS, ROWS), piece(WY_COLS, 64), piece(WZ_COLS, 64)
-
-    local[0].wait()
-    for i, off in ((0, 1), (1, -1)):
-        send(wy(x, y), wy(x, y), WX0 + i, at(0, off))
-    for i, off in ((0, 1), (1, -1)):
-        send(wz(x, z), wz(x, z), WX0 + 2 + i, at(0, off))
-
-    for c in small:
-        c.wait()
-    tkown[0:TAPS, :] = taps_in[...].astype(F32)
-    tkown[TAPS : TAPS + 1, :] = gain_in[...].astype(F32)
-    tkall[s] = tkown[...].astype(BF16)
-
-    def send_taps(r):
-        copy(tkall.at[s], tkall.at[s], TAP0 + r, {"sp": (s + r + 1) % NSP, "dp": d}).start()
-
-    loop(NSP - 1, send_taps)
-
     local[1].wait()
     local[2].wait()
 
@@ -237,10 +209,40 @@
             HALO0 + n,
             {"sp": (s + 1) % NSP, "dp": d},
         )
+    pl.semaphore_wait(barrier, NSP - 1 + NDP - 1 + 6)
+
+    def piece(cols, size):
+        def at_quarter(xx, quarter, h=None):
+            n, first = (size, quarter * size) if h is None else (size // 2, quarter * size + h * (size // 2))
+            return wg.at[xx, pl.ds(pl.multiple_of(first, n), n), pl.ds(*cols)]
+
+        return at_quarter
+
+    wx, wy, wz = piece(WX_COLS, ROWS), piece(WY_COLS, 64), piece(WZ_COLS, 64)
+
+    local[0].wait()
+    for i, off in ((0, 1), (1, -1)):
+        send(wy(x, y), wy(x, y), WX0 + i, at(0, off))
+    for i, off in ((0, 1), (1, -1)):
+        send(wz(x, z), wz(x, z), WX0 + 2 + i, at(0, off))
 
     @pl.when(s < NSP - 1)
     def _():
         halo_copy(0).start()
+
+    for c in small:
+        c.wait()
+    tkown[0:TAPS, :] = taps_in[...].astype(F32)
+    tkown[TAPS : TAPS + 1, :] = gain_in[...].astype(F32)
+    tkall[s] = tkown[...].astype(BF16)
+
+    def send_taps(r):
+        copy(tkall.at[s], tkall.at[s], TAP0 + r, {"sp": (s + r + 1) % NSP, "dp": d}).start()
+
+    loop(NSP - 1, send_taps)
+
+    @pl.when(s < NSP - 1)
+    def _():
         halo_copy(1).start()
 
     local[3].wait()
@@ -414,12 +416,12 @@
     blocks = (pa, pb, pc)
     half = lanes(q, HALF)
 
-    def outer(g, zr, i):
+    def outer(g, zr):
         p = lax.dot_general(
-            act[:, lanes(2 * g + i, 256)], cotp[:, half], (((0,), (0,)), ((), ())), preferred_element_type=F32
+            act[:, lanes(g, 512)], cotp[:, half], (((0,), (0,)), ((), ())), preferred_element_type=F32
         ).astype(BF16)
-        for n in range(8):
-            yy, xx = i * 2 + n // 4, n % 4
+        for n in range(16):
+            yy, xx = n // 4, n % 4
             part = p[32 * n : 32 * n + 32]
             pa[xx, yy, zr] = part[:, 0:384]
             pb[yy, zr, xx] = part[:, 384:640]
@@ -443,7 +445,7 @@
 
     for pos, (g, zr) in enumerate(zip(groups, order)):
         got(act.at[rows(1 - q, ROWS), lanes(g, 512)], ACT0 + pos)
-        loop(2, lambda i, g=g, zr=zr: outer(g, zr, i))
+        outer(g, zr)
         if pos == 1:
             across_on(2, left, 0)
             across_on(1, right, 1)

time: 58.8 us -> 58.2 us (0.990)
  no operation moved by 1% of the time
where the time goes in v5:
time: 58.2 us; the launch traced here: 58.1 us
  Pallas kernels  57.5 us (99%)
  between operations  0.64 us (1%)
    pallas_call x1, Pallas kernels, shards(): pl.pallas_call(kernel, out_shape=(jax.ShapeDtypeStruct((ROWS, D), BF16),...  55 us
    pallas_call x1, Pallas kernels, shards(): pl.pallas_call(place, out_shape=(jax.ShapeDtypeStruct((ROWS, D), BF16), j...  2.5 us

profile of v5, /device:TPU:1, one launch (start us, length us, event | category | flops | bytes accessed | tf_op | source)
XLA Modules:
  0.0 58.1 jit_solution(14653180070103759263)
XLA Ops:
  0.6 55.0 %shard_map.101 = (bf16[256,2048]{1,0:T(8,128)(2,1)}, bf16[256,2048]{1,0:T(8,128)(2,1)}, f32[16,2048]{1,0:T(8,128)}, f32[32,128]{1,0:T(8,128)}) custom-call(bf16[256,2048]{1,0:T(8,128)(2,1)} %bitcast.7, bf16[256,2048]{1,0:T(8,128)(2,1)} %bitcast.8, bf16[256,2048]{1,0:T(8,128)(2,1)} %bitcast.9, bf16[256,2048]{1,0:T(8,128)(2,1)} %w_hbm.1, ...), custom_call_target="tpu_custom_call" | custom-call | tf_op jit(solution)/shard_map/pallas_call | solution.py:826
  55.6 2.5 %shard_map.102 = (bf16[256,2048]{1,0:T(8,128)(2,1)}, bf16[256,2048]{1,0:T(8,128)(2,1)}, f32[16,2048]{1,0:T(8,128)}, f32[31,128]{1,0:T(8,128)}, f32[1,128]{1,0:T(1,128)}) custom-call(bf16[256,2048]{1,0:T(8,128)(2,1)} %get-tuple-element.14.gv_in, bf16[256,2048]{1,0:T(8,128)(2,1)} %get-tuple-element.15.gg_in, f32[16,2048]{1,0:T(8,128)} %get-tuple-element.16.ow_in, ...), custom_call_target="tpu_custom_call" | custom-call | tf_op jit(solution)/shard_map/pallas_call | solution.py:842

commit v6 on v5

--- a/solution.py
+++ b/solution.py
@@ -760,16 +760,16 @@
     small.start()
     for c in ins:
         c.start()
+    small.wait()
+    tp[...] = gk[0:TAPS, :]
+    gn[...] = gk[TAPS : TAPS + 1, :]
+    tiny = [pltpu.make_async_copy(tp, taps_hbm, ssem.at[9]), pltpu.make_async_copy(gn, gain_hbm, ssem.at[10])]
+    for o in tiny:
+        o.start()
     for c, o in zip(ins, outs):
         c.wait()
         o.start()
-    small.wait()
-    tp[...] = gk[0:TAPS, :]
-    gn[...] = gk[TAPS : TAPS + 1, :]
-    outs.append(pltpu.make_async_copy(tp, taps_hbm, ssem.at[9]))
-    outs.append(pltpu.make_async_copy(gn, gain_hbm, ssem.at[10]))
-    outs[-2].start()
-    outs[-1].start()
+    outs = outs + tiny
     for o in outs:
         o.wait()
 

time: 58.2 us -> 58.3 us (level)
  no operation moved by 1% of the time
where the time goes in v6:
time: 58.3 us; the launch traced here: 58.1 us
  Pallas kernels  57.5 us (99%)
  between operations  0.64 us (1%)
    pallas_call x1, Pallas kernels, shards(): pl.pallas_call(kernel, out_shape=(jax.ShapeDtypeStruct((ROWS, D), BF16),...  55 us
    pallas_call x1, Pallas kernels, shards(): pl.pallas_call(place, out_shape=(jax.ShapeDtypeStruct((ROWS, D), BF16), j...  2.5 us

profile of v6, /device:TPU:1, one launch (start us, length us, event | category | flops | bytes accessed | tf_op | source)
XLA Modules:
  0.0 58.1 jit_solution(9374491886011035094)
XLA Ops:
  0.6 55.0 %shard_map.101 = (bf16[256,2048]{1,0:T(8,128)(2,1)}, bf16[256,2048]{1,0:T(8,128)(2,1)}, f32[16,2048]{1,0:T(8,128)}, f32[32,128]{1,0:T(8,128)}) custom-call(bf16[256,2048]{1,0:T(8,128)(2,1)} %bitcast.7, bf16[256,2048]{1,0:T(8,128)(2,1)} %bitcast.8, bf16[256,2048]{1,0:T(8,128)(2,1)} %bitcast.9, bf16[256,2048]{1,0:T(8,128)(2,1)} %w_hbm.1, ...), custom_call_target="tpu_custom_call" | custom-call | tf_op jit(solution)/shard_map/pallas_call | solution.py:826
  55.6 2.5 %shard_map.102 = (bf16[256,2048]{1,0:T(8,128)(2,1)}, bf16[256,2048]{1,0:T(8,128)(2,1)}, f32[16,2048]{1,0:T(8,128)}, f32[31,128]{1,0:T(8,128)}, f32[1,128]{1,0:T(1,128)}) custom-call(bf16[256,2048]{1,0:T(8,128)(2,1)} %get-tuple-element.14.gv_in, bf16[256,2048]{1,0:T(8,128)(2,1)} %get-tuple-element.15.gg_in, f32[16,2048]{1,0:T(8,128)} %get-tuple-element.16.ow_in, ...), custom_call_target="tpu_custom_call" | custom-call | tf_op jit(solution)/shard_map/pallas_call | solution.py:842
